TPU v7x, 256 devices: a whole 4x4x8 slice. The times are simulated.
256 devices in a mesh: sp: 64 (over z, y, core), tp: 4 (over x).
Axes of the slice: x: 4, y: 4, z: 8, core: 2. Of those that a mesh axis runs over, the one named last changes fastest.
Arguments:
- head_input_values: bfloat16 [24576, 4096], P('sp', 'tp'), may hold values from -6 to 6
- group_input_vectors: bfloat16 [24576, 1024], P('sp', 'tp'), may hold values from -6 to 6
- group_readout_vectors: bfloat16 [24576, 1024], P('sp', 'tp'), may hold values from -6 to 6
- output_gate_values: bfloat16 [24576, 4096], P('sp', 'tp'), may hold values from -6 to 6
- step_size_logits: float32 [24576, 64], P('sp', 'tp'), may hold values from -6 to 6
- extra_log_decay: float32 [24576, 64], P('sp', 'tp'), may hold values from -1.2 to 0
- head_input_filter: bfloat16 [4, 4096], P(None, 'tp'), may hold values from -3 to 3
- input_vector_filter: bfloat16 [4, 1024], P(None, 'tp'), may hold values from -3 to 3
- readout_vector_filter: bfloat16 [4, 1024], P(None, 'tp'), may hold values from -3 to 3
- step_size_bias: float32 [64], P('tp'), may hold values from -0.5 to 0.5
- head_rate_logarithm: float32 [64], P('tp'), may hold values from -20 to -1
- direct_path_weight: float32 [64], P('tp'), may hold values from 0 to 3
- group_norm_scale: bfloat16 [4096], P('tp'), may hold values from 0.099609375 to 1.8984375
- mixer_output_weight: bfloat16 [4096, 2048], P('tp'), may hold values from -0.09375 to 0.09375
- residual: bfloat16 [24576, 2048], P(('sp', 'tp')), may hold values from -6 to 6
- first_norm_scale: float32 [2048], replicated, may hold values from 0.1 to 1.9
- first_norm_bias: float32 [2048], replicated, may hold values from -1.5 to 1.5
- routes: int32 [24576, 2], P(('sp', 'tp')), may hold values from 0 to 63, all different within a row; in each aligned block of 96 rows (0 to 95, 96 to 191, ...) at most 5 rows name the same one
- routing_weight: float32 [24576, 2], P(('sp', 'tp')), may hold values from 0.1 to 0.9
- expert_gate_weight: bfloat16 [64, 2048, 1024], P('sp', None, 'tp'), may hold values from -0.125 to 0.125
- expert_up_weight: bfloat16 [64, 2048, 1024], P('sp', None, 'tp'), may hold values from -0.125 to 0.125
- expert_down_weight: bfloat16 [64, 2048, 1024], P('sp', None, 'tp'), may hold values from -0.1875 to 0.1875
- final_norm_scale: float32 [2048], replicated, may hold values from 0.1 to 1.9
- final_norm_bias: float32 [2048], replicated, may hold values from -1.5 to 1.5
Outputs:
- final: bfloat16 [24576, 2048], P(('sp', 'tp'))
Inputs may be any that keep to these rules, and one draw needn't show every extreme that they name: `routes`: in the rows of one device no expert is named more than 5 times.
All inputs are finite; a program needn't handle non-finite values.
Results may differ from a plain program's by a relative error of at most 0.012.
Values may be sent and summed in bfloat16 or wider, within the bound.
A program may use at most 128 MiB of HBM per device.

v0:
```python
import jax
import jax.numpy as jnp
from jax import lax
from jax.sharding import Mesh
from jax.sharding import PartitionSpec as P

HEAD_DIM = 64
STATE_WIDTH = 128
BLOCK_LENGTH = 128
SP = ("sp_0", "sp_1", "sp_2")
SP_TP = ("sp_0", "sp_1", "sp_2", "tp")


EPS = 1e-05
ALPHA = 8.0**0.25


def from_behind(block, axis, distance):
    devices = range(lax.axis_size(axis))
    route = [(i - distance, i) for i in devices if i - distance in devices]
    return lax.ppermute(block, axis, route)


def filled_with(value, identity):
    return jax.tree.map(
        lambda a, e: jnp.broadcast_to(jnp.asarray(e, a.dtype), a.shape), value, identity
    )


def prefix_by_axis(value, axes, combine, identity):
    before = start = filled_with(value, identity)
    so_far = value
    for axis in reversed(axes):
        peers, place = (lax.axis_size(axis), lax.axis_index(axis))
        pieces = jax.tree.map(
            lambda part, kind: lax.all_gather(part.astype(kind), axis),
            so_far,
            (jnp.bfloat16, jnp.bfloat16),
        )
        inside, so_far = (start, start)
        for k in range(peers):
            passed = k < place
            so_far = combine(
                so_far, jax.tree.map(lambda part, own: part[k].astype(own.dtype), pieces, value)
            )
            inside = jax.tree.map(lambda new, old: jnp.where(passed, new, old), so_far, inside)
        before = combine(inside, before)
    return before


def split_up(value, dim, peers):
    before, after = (value.shape[:dim], value.shape[dim + 1 :])
    return jnp.moveaxis(value.reshape(*before, peers, -1, *after), dim, 0)


def summed_on_arrival(value, axis, dim):
    peers = lax.axis_size(axis)
    parts = lax.all_to_all(split_up(value, dim, peers), axis, 0, 0, tiled=True)
    return jnp.sum(parts.astype(jnp.float32), axis=0)


def side_by_side(arrays, axis, dim, along):
    widths = [a.shape[along] for a in arrays]
    both = jnp.concatenate(arrays, axis=along)
    filled = lax.all_gather(both, axis, axis=dim, tiled=True)
    return tuple(jnp.split(filled, [sum(widths[:k]) for k in range(1, len(widths))], axis=along))


def layer_norm(values, gain_row, bias_row):
    mean_value = jnp.mean(values, axis=-1, keepdims=True)
    centred = values - mean_value
    spread = jnp.mean(centred * centred, axis=-1, keepdims=True)
    return centred * lax.rsqrt(spread + EPS) * gain_row + bias_row


def conv_silu(raw_rows, tail_rows, tap_weights):
    full_rows = jnp.concatenate([tail_rows, raw_rows], axis=0).astype(jnp.float32)
    weights = tap_weights.astype(jnp.float32)
    length = raw_rows.shape[0]
    summed_output = jnp.zeros((length, raw_rows.shape[1]), jnp.float32)
    for offset in range(tap_weights.shape[0]):
        summed_output = summed_output + weights[offset] * full_rows[offset : offset + length]
    return jax.nn.silu(summed_output)


def block_pass(state_now, input_blocks):
    step_scaled_inputs, decay_logarithm, inputs_b, reads_c = input_blocks
    running = jnp.cumsum(decay_logarithm, axis=0)
    running_t = jnp.moveaxis(running, 0, -1)
    length = decay_logarithm.shape[0]
    causal = jnp.arange(length)[:, None] >= jnp.arange(length)[None, :]
    spread_log = jnp.where(causal, running_t[..., :, None] - running_t[..., None, :], -jnp.inf)
    decay_factors = jnp.exp(spread_log)
    decay_products = jnp.einsum("tgn,sgn->gts", reads_c, inputs_b)
    within_block_output = jnp.einsum(
        "zmka,azmo->kzmo", decay_products[:, None] * decay_factors, step_scaled_inputs
    )
    carried_in = jnp.einsum("tgn,grpn->tgrp", reads_c, state_now) * jnp.exp(running)[..., None]
    to_end = jnp.exp(running_t[..., -1:] - running_t)
    added = jnp.einsum("sgn,grs,sgrp->grpn", inputs_b, to_end, step_scaled_inputs)
    state_next = jnp.exp(running_t[..., -1])[..., None, None] * state_now + added
    return (state_next, within_block_output + carried_in)


def chain_states(earlier, later):
    return (earlier[0] + later[0], jnp.exp(later[0])[..., None, None] * earlier[1] + later[1])


def slot_layout(block_routes, capacity, experts):
    flat_routes = block_routes.reshape(-1)
    matches = (flat_routes[:, None] == jnp.arange(experts, dtype=jnp.int32)[None, :]).astype(
        jnp.int32
    )
    before = jnp.cumsum(matches, axis=0) - matches
    return flat_routes * capacity + jnp.sum(before * matches, axis=1)


def expert_hidden(arrived, weight_gate, weight_up):
    local_count = weight_gate.shape[0]
    grouped = arrived.reshape(-1, local_count, arrived.shape[1], arrived.shape[2])
    gate_part = jnp.einsum(
        "send,edf->senf", grouped, weight_gate, preferred_element_type=jnp.float32
    )
    up_part = jnp.einsum("send,edf->senf", grouped, weight_up, preferred_element_type=jnp.float32)
    return (jax.nn.silu(gate_part) * up_part).astype(jnp.bfloat16)


def expert_output(hidden, weight_down):
    result = jnp.einsum("senf,edf->send", hidden, weight_down, preferred_element_type=jnp.float32)
    return result.reshape(-1, result.shape[2], result.shape[3])


def shards(
    head_input_values,
    group_input_vectors,
    group_readout_vectors,
    output_gate_values,
    step_size_logits,
    extra_log_decay,
    head_input_filter,
    input_vector_filter,
    readout_vector_filter,
    step_size_bias,
    head_rate_logarithm,
    direct_path_weight,
    group_norm_scale,
    mixer_output_weight,
    residual,
    first_norm_scale,
    first_norm_bias,
    routes,
    routing_weight,
    expert_gate_weight,
    expert_up_weight,
    expert_down_weight,
    final_norm_scale,
    final_norm_bias,
):
    length = head_input_values.shape[0]
    margin = head_input_filter.shape[0] - 1
    tail_x, tail_b, tail_c = from_behind(
        (
            head_input_values[length - margin :],
            group_input_vectors[length - margin :],
            group_readout_vectors[length - margin :],
        ),
        SP,
        1,
    )
    conv_x = conv_silu(head_input_values, tail_x, head_input_filter)
    conv_b = conv_silu(group_input_vectors, tail_b, input_vector_filter)
    conv_c = conv_silu(group_readout_vectors, tail_c, readout_vector_filter)
    heads_here = head_input_values.shape[1] // HEAD_DIM
    groups_here = group_input_vectors.shape[1] // STATE_WIDTH
    repeat_count = heads_here // groups_here
    step_sizes = jax.nn.softplus(step_size_logits + step_size_bias)
    decay_logarithm = -step_sizes * jnp.exp(head_rate_logarithm) + extra_log_decay
    heads_x = conv_x.reshape(length, groups_here, repeat_count, HEAD_DIM)
    step_scaled_inputs = heads_x * step_sizes.reshape(length, groups_here, repeat_count)[..., None]
    decay_heads = decay_logarithm.reshape(length, groups_here, repeat_count)
    inputs_b = conv_b.reshape(length, groups_here, STATE_WIDTH)
    reads_c = conv_c.reshape(length, groups_here, STATE_WIDTH)
    block_list = length // BLOCK_LENGTH
    start_state = jnp.zeros((groups_here, repeat_count, HEAD_DIM, STATE_WIDTH), jnp.float32)
    end_state, within_block_output = lax.scan(
        block_pass,
        start_state,
        (
            step_scaled_inputs.reshape(
                block_list, BLOCK_LENGTH, groups_here, repeat_count, HEAD_DIM
            ),
            decay_heads.reshape(block_list, BLOCK_LENGTH, groups_here, repeat_count),
            inputs_b.reshape(block_list, BLOCK_LENGTH, groups_here, STATE_WIDTH),
            reads_c.reshape(block_list, BLOCK_LENGTH, groups_here, STATE_WIDTH),
        ),
    )
    total_decay = jnp.sum(decay_heads, axis=0)
    identity = (jnp.zeros_like(total_decay), jnp.zeros_like(end_state))
    earlier_part = prefix_by_axis((total_decay, end_state), SP, chain_states, identity)
    incoming = earlier_part[1]
    device_running = jnp.cumsum(decay_heads, axis=0)
    readout = jnp.einsum("tgn,grpn->tgrp", reads_c, incoming) * jnp.exp(device_running)[..., None]
    ssm_out = (
        within_block_output.reshape(length, groups_here, repeat_count, HEAD_DIM)
        + readout
        + direct_path_weight.reshape(groups_here, repeat_count)[None, :, :, None] * heads_x
    )
    gated = ssm_out.reshape(length, -1) * jax.nn.silu(output_gate_values.astype(jnp.float32))
    grouped = gated.reshape(length, groups_here, -1)
    normed = grouped * lax.rsqrt(jnp.mean(grouped * grouped, axis=-1, keepdims=True) + EPS)
    mixer_rows = (normed.reshape(length, -1) * group_norm_scale.astype(jnp.float32)).astype(
        jnp.bfloat16
    )
    rows_here = residual.shape[0]
    mixed = summed_on_arrival(
        jnp.dot(mixer_rows, mixer_output_weight, preferred_element_type=jnp.float32).astype(
            jnp.bfloat16
        ),
        "tp",
        0,
    )
    middle = layer_norm(
        ALPHA * residual.astype(jnp.float32) + mixed, first_norm_scale, first_norm_bias
    ).astype(jnp.bfloat16)
    top_count = routes.shape[1]
    width = middle.shape[1]
    experts = expert_gate_weight.shape[0] * lax.axis_size(SP)
    capacity = max(2, rows_here * top_count * 5 // (3 * experts))
    slot_ids = slot_layout(routes, capacity, experts)
    owners = jnp.repeat(jnp.arange(rows_here, dtype=jnp.int32), top_count)
    source = jnp.full((experts * capacity,), rows_here, jnp.int32).at[slot_ids].set(owners)
    padded = jnp.concatenate([middle, jnp.zeros((1, width), jnp.bfloat16)], axis=0)
    outgoing = padded[source].reshape(experts, capacity, width)
    whole_gate, whole_up, whole_down = side_by_side(
        (expert_gate_weight, expert_up_weight, expert_down_weight), "tp", 2, 0
    )
    hidden = expert_hidden(
        lax.all_to_all(outgoing, SP, split_axis=0, concat_axis=0, tiled=True), whole_gate, whole_up
    )
    answers = expert_output(hidden, whole_down).astype(jnp.bfloat16)
    returned = lax.all_to_all(answers, SP, split_axis=0, concat_axis=0, tiled=True)
    picked = (
        returned.reshape(-1, width)[slot_ids]
        .astype(jnp.float32)
        .reshape(rows_here, top_count, width)
    )
    ffn = jnp.sum(picked * routing_weight[..., None], axis=1)
    return layer_norm(
        ALPHA * middle.astype(jnp.float32) + ffn, final_norm_scale, final_norm_bias
    ).astype(jnp.bfloat16)


def solution(mesh):
    split = Mesh(mesh.devices.reshape(8, 4, 2, mesh.shape["tp"]), ("sp_0", "sp_1", "sp_2", "tp"))
    placed = (
        P(SP, "tp"),
        P(SP, "tp"),
        P(SP, "tp"),
        P(SP, "tp"),
        P(SP, "tp"),
        P(SP, "tp"),
        P(None, "tp"),
        P(None, "tp"),
        P(None, "tp"),
        P("tp"),
        P("tp"),
        P("tp"),
        P("tp"),
        P("tp", None),
        P(SP_TP, None),
        P(),
        P(),
        P(SP_TP, None),
        P(SP_TP, None),
        P(SP, None, "tp"),
        P(SP, None, "tp"),
        P(SP, None, "tp"),
        P(),
        P(),
    )
    return jax.shard_map(
        shards, mesh=split, in_specs=placed, out_specs=P(SP_TP, None), check_vma=False
    )
```

profile of v0, /device:TPU:1, one launch (start us, length us, event | category | flops | bytes accessed | tf_op | source)
XLA Modules:
  0.0 396.6 jit_solution(11025642554368086106)
XLA Ops:
  7.3 4.6 %collective-permute-start = (bf16[3,1024]{1,0:T(4,128)(2,1)S(1)}, bf16[3,1024]{1,0:T(4,128)(2,1)S(1)}, u32[]{:S(2)}, u32[]{:S(2)}) collective-permute-start(bf16[3,1024]{1,0:T(4,128)(2,1)S(1)} %slice.185), channel_id=1, source_target_pairs={{0,4},{4,8},{8,12},{12,16},{16,20},{20,24},{24,28},{28,32},{32,36}... | collective-permute-start | bytes 18440 | tf_op jit(solution)/shard_map/ppermute | solution.py:21
  15.2 3.6 collective-permute-start.1
  30.1 2.5 reshape.382
  34.4 53.9 %while.13 = (s32[]{:T(128)}, f32[2,8,64,128]{3,2,1,0:T(8,128)S(1)}, f32[3,128,2,8,64]{1,0,4,3,2:T(4,128)}, f32[3,128,2,8]{1,0,3,2:T(4,128)S(1)}, f32[3,128,2,8,6...) while((s32[]{:T(128)}, f32[2,8,64,128]{3,2,1,0:T(8,128)S(1)}, ...), condition=%wide.region_2.3_spmd.clone, body=%wide.region_0.2_spmd.clone.sunk | while | flops 111034368 | bytes 7258616 | solution.py:185
  38.1 13.8 %dynamic_update_slice.6 = f32[3,128,2,8,64]{1,0,4,3,2:T(4,128)} dynamic-update-slice(f32[3,128,2,8,64]{1,0,4,3,2:T(4,128)} %get-tuple-element.209, f32[1,128,2,8,64]{1,0,4,3,2:T(1,128)S(1)} %bitcast.346, s32[]{:T(128)} %get-tuple-element.207, s32[]{:T(128)} %constant.42.clone.1..sunk, s32[]{:T(128)} %constant.42.clone.1..sunk, s32[]{:T(128)} %constant.42.clone.1..sunk, s32[]{:T(128)} %constant.42.clone.1..sunk) | dynamic-update-slice | bytes 1048580 | tf_op jit(solution)/shard_map/while/body/jit(dynamic_update_index_in_dim)/dynamic_update_slice | solution.py:185
  53.3 2.2 constant_dynamic-slice_fusion.7
  56.0 13.8 %dynamic_update_slice.6 = f32[3,128,2,8,64]{1,0,4,3,2:T(4,128)} dynamic-update-slice(f32[3,128,2,8,64]{1,0,4,3,2:T(4,128)} %get-tuple-element.209, f32[1,128,2,8,64]{1,0,4,3,2:T(1,128)S(1)} %bitcast.346, s32[]{:T(128)} %get-tuple-element.207, s32[]{:T(128)} %constant.42.clone.1..sunk, s32[]{:T(128)} %constant.42.clone.1..sunk, s32[]{:T(128)} %constant.42.clone.1..sunk, s32[]{:T(128)} %constant.42.clone.1..sunk) | dynamic-update-slice | bytes 1048580 | tf_op jit(solution)/shard_map/while/body/jit(dynamic_update_index_in_dim)/dynamic_update_slice | solution.py:185
  74.0 13.8 %dynamic_update_slice.6 = f32[3,128,2,8,64]{1,0,4,3,2:T(4,128)} dynamic-update-slice(f32[3,128,2,8,64]{1,0,4,3,2:T(4,128)} %get-tuple-element.209, f32[1,128,2,8,64]{1,0,4,3,2:T(1,128)S(1)} %bitcast.346, s32[]{:T(128)} %get-tuple-element.207, s32[]{:T(128)} %constant.42.clone.1..sunk, s32[]{:T(128)} %constant.42.clone.1..sunk, s32[]{:T(128)} %constant.42.clone.1..sunk, s32[]{:T(128)} %constant.42.clone.1..sunk) | dynamic-update-slice | bytes 1048580 | tf_op jit(solution)/shard_map/while/body/jit(dynamic_update_index_in_dim)/dynamic_update_slice | solution.py:185
  88.3 2.3 all-gather
  91.7 8.0 %all_gather.30 = bf16[4,2,8]{2,1,0:T(2,128)(2,1)S(1)} all-gather(bf16[1,2,8]{2,1,0:T(2,128)(2,1)S(1)} %get-tuple-element.145), channel_id=1, replica_groups=mesh['sp_0'=8,'sp_1'=4,'sp_2'=2,'tp'=4] {'sp_1'}, dimensions={0}, use_global_device_ids=true | all-gather | bytes 160 | tf_op jit(solution)/shard_map/all_gather | solution.py:36
  99.7 18.1 %all-gather.5.cloned.1.call-done = bf16[4,2,8,64,128]{4,3,2,1,0:T(8,128)(2,1)} async-done(((bf16[1,2,8,64,128]{4,3,2,1,0:T(8,128)(2,1)}), bf16[4,2,8,64,128]{4,3,2,1,0:T(8,128)(2,1)}) %all-gather.5.cloned.1.call-update) | async-done | bytes 1048592 | tf_op jit(solution)/shard_map/all_gather | solution.py:36
  117.8 2.2 fusion.75
  120.1 3.6 pad_maximum_fusion
  126.6 13.9 %all_gather.31 = bf16[8,2,8]{2,1,0:T(2,128)(2,1)S(1)} all-gather(bf16[1,2,8]{2,1,0:T(2,128)(2,1)S(1)} %get-tuple-element.132), channel_id=1, replica_groups=mesh['sp_0'=8,'sp_1'=4,'sp_2'=2,'tp'=4] {'sp_0'}, dimensions={0}, use_global_device_ids=true | all-gather | bytes 288 | tf_op jit(solution)/shard_map/all_gather | solution.py:36
  140.6 3.9 reshape.383
  144.6 14.6 %all-gather.7.cloned.1.call-done = bf16[8,2,8,64,128]{4,3,2,1,0:T(8,128)(2,1)} async-done(((bf16[1,2,8,64,128]{4,3,2,1,0:T(8,128)(2,1)}), bf16[8,2,8,64,128]{4,3,2,1,0:T(8,128)(2,1)}) %all-gather.7.cloned.1.call-update) | async-done | bytes 2097168 | tf_op jit(solution)/shard_map/all_gather | solution.py:36
  159.2 4.9 %fusion.43 = f32[384,2,8,64]{0,3,2,1:T(8,128)} fusion(f32[384,2,8,64]{0,3,2,1:T(8,128)} %reshape.383, f32[384,2,8,64]{0,3,2,1:T(8,128)S(1)} %bitcast.350, f32[2,8]{1,0:T(2,128)S(1)} %mul.557, f32[384,2,8]{0,2,1:T(8,128)S(1)} %bitcast_bitcast_fusion.1, bf16[384,2,128,1]{2,1,0,3:T(2,128)(2,1)S(1)} %bitcast.354, ...), kind=kOutput, calls=%fused_computation.69 | convolution fusion | flops 109707264 | bytes 8610894 | tf_op jit(solution)/shard_map/tgn,grpn->tgrp/dot_general | solution.py:202
  167.6 2.6 mul.563
  173.3 3.2 convolution_convert_fusion
  176.5 4.0 %all-to-all-start = ((bf16[4,96,2048]{2,1,0:T(8,128)(2,1)}), bf16[4,96,2048]{2,1,0:T(8,128)(2,1)S(1)}, u32[]{:S(2)}, u32[]{:S(2)}) async-start(bf16[4,96,2048]{2,1,0:T(8,128)(2,1)} %bitcast.50), calls=%async_computation | async-start | bytes 3145728 | tf_op jit(solution)/shard_map/all_to_all | solution.py:58
  182.5 34.0 %all-to-all-done = bf16[4,96,2048]{2,1,0:T(8,128)(2,1)S(1)} async-done(((bf16[4,96,2048]{2,1,0:T(8,128)(2,1)}), bf16[4,96,2048]{2,1,0:T(8,128)(2,1)S(1)}, u32[]{:S(2)}, u32[]{:S(2)}) %all-to-all-start) | async-done | bytes 1572896 | tf_op jit(solution)/shard_map/all_to_all | solution.py:58
  217.8 3.0 gather_fusion
  220.8 2.4 reshape.396
  223.1 63.3 %all_to_all.15 = bf16[64,5,2048]{2,1,0:T(8,128)(2,1)} all-to-all(bf16[64,5,2048]{2,1,0:T(8,128)(2,1)S(1)} %reshape.396), channel_id=1, replica_groups=mesh['sp_0'=8,'sp_1'=4,'sp_2'=2,'tp'=4] {'sp_0','sp_1','sp_2'}, dimensions={0} | all-to-all | bytes 2621440 | tf_op jit(solution)/shard_map/all_to_all | solution.py:238
  286.5 18.1 %all-gather.9.cloned.1.call-done = bf16[3,2048,1024]{2,1,0:T(8,128)(2,1)} async-done(((bf16[3,2048,256]{2,1,0:T(8,128)(2,1)}), bf16[3,2048,1024]{2,1,0:T(8,128)(2,1)}) %all-gather.9.cloned.1.call-update) | async-done | bytes 12582928 | tf_op jit(solution)/shard_map/all_gather | solution.py:65
  304.6 5.8 %fusion.44 = f32[64,1,5,1024]{3,0,2,1:T(8,128)} fusion(bf16[3,2048,1024]{2,1,0:T(8,128)(2,1)} %all-gather.9.cloned.1.call-done, bf16[64,5,2048]{2,1,0:T(8,128)(2,1)} %all_to_all.15), kind=kOutput, calls=%fused_computation.73 | convolution fusion | flops 1342177280 | bytes 7602176 | tf_op jit(solution)/shard_map/send,edf->senf/dot_general | solution.py:121
  310.4 8.1 %fusion.34 = bf16[64,5,2048]{2,0,1:T(8,128)(2,1)} fusion(bf16[3,2048,1024]{2,1,0:T(8,128)(2,1)} %all-gather.9.cloned.1.call-done, f32[64,1,5,1024]{3,0,2,1:T(8,128)} %fusion.44, bf16[64,5,2048]{2,1,0:T(8,128)(2,1)S(1)} %copy-done.2), kind=kOutput, calls=%fused_computation.53 | convolution fusion | flops 2686976000 | bytes 12320768 | tf_op jit(solution)/shard_map/senf,edf->send/dot_general | solution.py:129
  318.5 3.4 copy.132
  321.9 9.9 %all-to-all-start.2 = ((bf16[64,5,2048]{2,1,0:T(8,128)(2,1)}), bf16[64,5,2048]{2,1,0:T(8,128)(2,1)}, u32[]{:S(2)}, u32[]{:S(2)}) async-start(bf16[64,5,2048]{2,1,0:T(8,128)(2,1)} %copy.132), calls=%async_computation.2 | async-start | bytes 4194304 | tf_op jit(solution)/shard_map/all_to_all | solution.py:241
  331.9 49.5 %all-to-all-done.2 = bf16[64,5,2048]{2,1,0:T(8,128)(2,1)} async-done(((bf16[64,5,2048]{2,1,0:T(8,128)(2,1)}), bf16[64,5,2048]{2,1,0:T(8,128)(2,1)}, u32[]{:S(2)}, u32[]{:S(2)}) %all-to-all-start.2) | async-done | bytes 1310752 | tf_op jit(solution)/shard_map/all_to_all | solution.py:241
  381.4 2.6 reshape.399
  386.1 2.3 multiply_reduce_fusion
  (171 shorter events, 44.7 us)
Async XLA Ops:
  6.5 19.6 %copy-start.7 = (bf16[384,256]{1,0:T(8,128)(2,1)S(1)}, bf16[384,256]{1,0:T(8,128)(2,1)}, u32[]{:S(2)}) copy-start(bf16[384,256]{1,0:T(8,128)(2,1)} %param.27) | copy-start | bytes 589828
  6.5 111.2 %all-gather.5.cloned.1.call-start = ((), (), s32[]{:S(2)}) async-start(), calls=%async_computation.3 | async-start | bytes 1310720 | tf_op jit(solution)/shard_map/all_gather | solution.py:36
  7.3 19.3 %collective-permute-start = (bf16[3,1024]{1,0:T(4,128)(2,1)S(1)}, bf16[3,1024]{1,0:T(4,128)(2,1)S(1)}, u32[]{:S(2)}, u32[]{:S(2)}) collective-permute-start(bf16[3,1024]{1,0:T(4,128)(2,1)S(1)} %slice.185), channel_id=1, source_target_pairs={{0,4},{4,8},{8,12},{12,16},{16,20},{20,24},{24,28},{28,32},{32,36}... | collective-permute-start | bytes 18440 | tf_op jit(solution)/shard_map/ppermute | solution.py:21
  12.6 12.3 %collective-permute-start.2 = (bf16[3,256]{1,0:T(4,128)(2,1)S(1)}, bf16[3,256]{1,0:T(4,128)(2,1)S(1)}, u32[]{:S(2)}, u32[]{:S(2)}) collective-permute-start(bf16[3,256]{1,0:T(4,128)(2,1)S(1)} %slice.203), channel_id=1, source_target_pairs={{0,4},{4,8},{8,12},{12,16},{16,20},{20,24},{24,28},{28,32},{32,36}... | collective-permute-start | bytes 4616 | tf_op jit(solution)/shard_map/ppermute | solution.py:21
  15.2 11.0 %collective-permute-start.1 = (bf16[3,256]{1,0:T(4,128)(2,1)S(1)}, bf16[3,256]{1,0:T(4,128)(2,1)S(1)}, u32[]{:S(2)}, u32[]{:S(2)}) collective-permute-start(bf16[3,256]{1,0:T(4,128)(2,1)S(1)} %slice.194), channel_id=1, source_target_pairs={{0,4},{4,8},{8,12},{12,16},{16,20},{20,24},{24,28},{28,32},{32,36}... | collective-permute-start | bytes 4616 | tf_op jit(solution)/shard_map/ppermute | solution.py:21
  26.1 1.1 copy-start.4
  88.3 31.8 %copy-start.3 = (bf16[1,2048,256]{2,1,0:T(8,128)(2,1)S(1)}, bf16[1,2048,256]{2,1,0:T(8,128)(2,1)}, u32[]{:S(2)}) copy-start(bf16[1,2048,256]{2,1,0:T(8,128)(2,1)} %param.47) | copy-start | bytes 3145732
  91.6 67.5 %all-gather.7.cloned.1.call-start = ((), (), s32[]{:S(2)}) async-start(), calls=%async_computation.4 | async-start | bytes 2359296 | tf_op jit(solution)/shard_map/all_gather | solution.py:36
  120.0 184.6 %all-gather.9.cloned.1.call-start = ((), (), s32[]{:S(2)}) async-start(), calls=%async_computation.5 | async-start | bytes 15728640 | tf_op jit(solution)/shard_map/all_gather | solution.py:65
  123.6 2.0 copy-start.16
  123.6 2.0 copy-start.13
  123.6 2.0 copy-start.12
  140.6 18.5 %copy-start = (f32[384,1024]{0,1:T(8,128)S(1)}, f32[384,1024]{0,1:T(8,128)}, u32[]{:S(2)}) copy-start(f32[384,1024]{0,1:T(8,128)} %copy.112) | copy-start | bytes 4718596
  164.1 2.0 copy-start.5
  170.8 2.2 copy-start.15
  171.3 2.0 copy-start.6
  176.5 40.0 %all-to-all-start = ((bf16[4,96,2048]{2,1,0:T(8,128)(2,1)}), bf16[4,96,2048]{2,1,0:T(8,128)(2,1)S(1)}, u32[]{:S(2)}, u32[]{:S(2)}) async-start(bf16[4,96,2048]{2,1,0:T(8,128)(2,1)} %bitcast.50), calls=%async_computation | async-start | bytes 3145728 | tf_op jit(solution)/shard_map/all_to_all | solution.py:58
  180.5 36.3 %copy-start.1 = (bf16[96,2048]{1,0:T(8,128)(2,1)S(1)}, bf16[96,2048]{1,0:T(8,128)(2,1)}, u32[]{:S(2)}) copy-start(bf16[96,2048]{1,0:T(8,128)(2,1)} %param.40) | copy-start | bytes 1179652
  216.8 0.7 copy-start.8
  216.8 0.7 copy-start.9
  286.5 23.9 %copy-start.2 = (bf16[64,5,2048]{2,1,0:T(8,128)(2,1)S(1)}, bf16[64,5,2048]{2,1,0:T(8,128)(2,1)}, u32[]{:S(2)}) copy-start(bf16[64,5,2048]{2,1,0:T(8,128)(2,1)} %all_to_all.15) | copy-start | bytes 3932164
  321.9 9.9 %copy-start.14 = (f32[96,2]{0,1:T(2,128)S(1)}, f32[96,2]{0,1:T(2,128)}, u32[]{:S(2)}) copy-start(f32[96,2]{0,1:T(2,128)} %param.44) | copy-start | bytes 2308
  321.9 59.5 %all-to-all-start.2 = ((bf16[64,5,2048]{2,1,0:T(8,128)(2,1)}), bf16[64,5,2048]{2,1,0:T(8,128)(2,1)}, u32[]{:S(2)}, u32[]{:S(2)}) async-start(bf16[64,5,2048]{2,1,0:T(8,128)(2,1)} %copy.132), calls=%async_computation.2 | async-start | bytes 4194304 | tf_op jit(solution)/shard_map/all_to_all | solution.py:241
  388.4 0.7 copy-start.10
  388.4 0.7 copy-start.11
Sparse Core Ops, SparseCore 0:
  91.7 25.9 all-gather.4
  120.1 38.9 all-gather.6
  161.0 143.5 all-gather.8
where the time goes:
time: 399 us; the launch traced here: 397 us
  waiting for transfers between devices  134 us (34%)
  blocking collectives  89.3 us (22%)
  local copies, waits for them, and re-layouts  86.9 us (22%)
  matrix products  25.7 us (6%)
  starting transfers between devices  24 us (6%)
  other arithmetic  22.4 us (6%)
  between operations  13.6 us (3%)
    all_to_all x1, blocking collectives, shards(): lax.all_to_all(outgoing, SP, split_axis=0, concat_axis=0, tiled=True)  63.3 us
    all_to_all x1, waiting for transfers between devices, shards(): lax.all_to_all(answers, SP, split_axis=0, concat_axis=0, tiled=True)  49.5 us
    dynamic_update_slice x3, local copies, waits for them, and re-layouts, shards(): lax.scan(block_pass, start_state, (step_scaled_inputs.reshape(block_list,...  41.5 us
    all_to_all x1, waiting for transfers between devices, summed_on_arrival(): parts = lax.all_to_all(split_up(value, dim, peers), axis, 0, 0, tiled=True)  34 us
    all_gather x2, waiting for transfers between devices, prefix_by_axis(): lax.all_gather(part.astype(kind), axis)  32.7 us
    all_gather x4, blocking collectives, prefix_by_axis(): lax.all_gather(part.astype(kind), axis)  26 us
    all_gather x1, waiting for transfers between devices, side_by_side(): filled = lax.all_gather(both, axis, axis=dim, tiled=True)  18.1 us
    ppermute x3, starting transfers between devices, from_behind(): return lax.ppermute(block, axis, route)  10.1 us
  transfers between devices with their start and end apart: 8, of which 5 were waited for; matrix products, arithmetic and copies ran while one was open for 11% of the time, Pallas kernels for 0%

commit v1 on v0

v1 whole, which is shorter than its diff:
```python
import functools

import jax
import jax.numpy as jnp
from jax import lax
from jax.experimental import pallas as pl
from jax.experimental.pallas import tpu as pltpu
from jax.sharding import PartitionSpec as P

HEAD_DIM = 64
STATE_WIDTH = 128
BLOCK = 128
EPS = 1e-05
ALPHA = 8.0**0.25
F32 = jnp.float32
BF16 = jnp.bfloat16
VMEM_LIMIT = 62 * 1024 * 1024


def dot(a, b, dims=((1,), (0,)), precision=None):
    return lax.dot_general(
        a, b, (dims, ((), ())), preferred_element_type=F32, precision=precision
    )


def silu(v):
    return v * (1.0 / (1.0 + jnp.exp(-v)))


def layer_norm(values, gain_row, bias_row):
    mean_value = jnp.mean(values, axis=-1, keepdims=True)
    centred = values - mean_value
    spread = jnp.mean(centred * centred, axis=-1, keepdims=True)
    return centred * lax.rsqrt(spread + EPS) * gain_row + bias_row


def remote(src, dst, send, recv, sp=None, tp=None):
    target = {}
    if sp is not None:
        target["sp"] = sp
    if tp is not None:
        target["tp"] = tp
    return pltpu.make_async_remote_copy(
        src_ref=src,
        dst_ref=dst,
        send_sem=send,
        recv_sem=recv,
        device_id=target,
        device_id_type=pl.DeviceIdType.MESH,
    )


def pair_columns(values, pair, low_half):
    rows = values.shape[0]
    first = jnp.broadcast_to(values[:, 2 * pair : 2 * pair + 1], (rows, 128))
    second = jnp.broadcast_to(values[:, 2 * pair + 1 : 2 * pair + 2], (rows, 128))
    return jnp.where(low_half[:rows], first, second)


def mixer_kernel(
    n_sp,
    n_tp,
    x,
    b,
    c,
    gate,
    logits,
    extra,
    fx,
    fb,
    fc,
    bias,
    rate,
    direct,
    gns,
    wout,
    resid,
    n1s,
    n1b,
    mid,
    tail_x,
    tail_b,
    tail_c,
    ext_x,
    ext_b,
    ext_c,
    dec_src,
    dec_recv,
    sl_src,
    sl_recv,
    pf_src,
    pf_recv,
    xs,
    xw,
    cb,
    cc,
    ysg,
    ersg,
    added,
    rows_out,
    partial,
    arrived,
    tail_sems,
    dec_sems,
    sl_sems,
    pf_sems,
    tp_sems,
):
    me = lax.axis_index("sp")
    col = lax.axis_index("tp")
    length, width = x.shape
    n_blocks = length // BLOCK
    pairs = width // 128
    groups = b.shape[1] // STATE_WIDTH
    group_width = width // groups

    after = lax.rem(me + 1, n_sp)
    tails = [
        remote(v.at[pl.ds(length - 8, 8)], t, tail_sems.at[0, i], tail_sems.at[1, i], sp=after)
        for i, (v, t) in enumerate(((x, tail_x), (b, tail_b), (c, tail_c)))
    ]
    for copy in tails:
        copy.start()

    low_half = lax.broadcasted_iota(jnp.int32, (BLOCK, 128), 1) < 64
    row_id = lax.broadcasted_iota(jnp.int32, (BLOCK, BLOCK), 0)
    lane_id = lax.broadcasted_iota(jnp.int32, (BLOCK, BLOCK), 1)
    causal = row_id >= lane_id
    lower = causal.astype(F32)

    raw = logits[...] + bias[...]
    steps = jnp.maximum(raw, 0.0) + jnp.log(1.0 + jnp.exp(-jnp.abs(raw)))
    decay = -steps * jnp.exp(rate[...]) + extra[...]
    running = [
        dot(lower, decay[BLOCK * k : BLOCK * (k + 1)], precision=lax.Precision.HIGHEST)
        for k in range(n_blocks)
    ]
    totals = [r[BLOCK - 1 : BLOCK] for r in running]
    whole = functools.reduce(lambda p, q: p + q, totals)
    for j in range(pairs):
        dec_src[j] = pair_columns(whole, j, low_half)

    def send_decay(d, carry):
        target = lax.rem(me + d, n_sp)
        remote(
            dec_src.at[lax.rem(target, pairs)],
            dec_recv.at[d],
            dec_sems.at[0],
            dec_sems.at[1],
            sp=target,
        ).start()
        return carry

    own_decay = pltpu.make_async_copy(
        dec_src.at[lax.rem(me, pairs)], dec_recv.at[0], dec_sems.at[1]
    )
    own_decay.start()
    lax.fori_loop(1, n_sp, send_decay, 0)

    ext_x[8:, :] = x[...].astype(F32)
    ext_b[8:, :] = b[...].astype(F32)
    ext_c[8:, :] = c[...].astype(F32)
    for copy in tails:
        copy.wait()
    has_tail = (me > 0).astype(F32)
    ext_x[0:8, :] = tail_x[...].astype(F32) * has_tail
    ext_b[0:8, :] = tail_b[...].astype(F32) * has_tail
    ext_c[0:8, :] = tail_c[...].astype(F32) * has_tail

    def conv(ext, taps, k, j):
        lanes = slice(128 * j, 128 * (j + 1))
        total = None
        for i in range(4):
            start = BLOCK * k + 5 + i
            term = taps[i : i + 1, lanes].astype(F32) * ext[start : start + BLOCK, lanes]
            total = term if total is None else total + term
        return silu(total)

    for g in range(groups):
        for k in range(n_blocks):
            rows = slice(BLOCK * k, BLOCK * (k + 1))
            lanes = slice(128 * g, 128 * (g + 1))
            cb[rows, lanes] = conv(ext_b, fb, k, g).astype(BF16)
            cc[rows, lanes] = conv(ext_c, fc, k, g).astype(BF16)

    for k in range(n_blocks):
        rows = slice(BLOCK * k, BLOCK * (k + 1))
        block_steps = steps[rows]
        to_end = block_steps * jnp.exp(totals[k] - running[k])
        for j in range(pairs):
            lanes = slice(128 * j, 128 * (j + 1))
            value = conv(ext_x, fx, k, j)
            xs[rows, lanes] = (value * pair_columns(block_steps, j, low_half)).astype(BF16)
            xw[rows, lanes] = (value * pair_columns(to_end, j, low_half)).astype(BF16)
            ysg[rows, lanes] = value * pair_columns(direct[...], j, low_half)

    keep = [
        jnp.concatenate([pair_columns(jnp.exp(t), j, low_half) for j in range(pairs)], axis=1)
        for t in totals
    ]
    for g in range(groups):
        for k in range(n_blocks):
            rows = slice(BLOCK * k, BLOCK * (k + 1))
            added[k, :, group_width * g : group_width * (g + 1)] = dot(
                cb[rows, 128 * g : 128 * (g + 1)],
                xw[rows, group_width * g : group_width * (g + 1)],
                ((0,), (0,)),
            )
    for i in range(STATE_WIDTH // 16):
        for j in range(pairs):
            lanes = slice(128 * j, 128 * (j + 1))
            state = added[0, 16 * i : 16 * (i + 1), lanes]
            for k in range(1, n_blocks):
                state = keep[k][:, lanes] * state + added[k, 16 * i : 16 * (i + 1), lanes]
            sl_src[pairs * i + j] = state.astype(BF16)

    def send_slice(d, carry):
        target = lax.rem(me + d, n_sp)
        remote(sl_src.at[target], sl_recv.at[d], sl_sems.at[0], sl_sems.at[1], sp=target).start()
        return carry

    own_slice = pltpu.make_async_copy(sl_src.at[me], sl_recv.at[0], sl_sems.at[1])
    own_slice.start()
    lax.fori_loop(1, n_sp, send_slice, 0)

    for k in range(n_blocks):
        rows = slice(BLOCK * k, BLOCK * (k + 1))
        across = running[k].T
        grown = jnp.exp(running[k])
        for g in range(groups):
            lanes_g = slice(128 * g, 128 * (g + 1))
            products = dot(cc[rows, lanes_g], cb[rows, lanes_g], ((1,), (1,)))
            for j in range(g * pairs // groups, (g + 1) * pairs // groups):
                lanes = slice(128 * j, 128 * (j + 1))
                weighed = []
                for h in (2 * j, 2 * j + 1):
                    spread = running[k][:, h : h + 1] - across[h : h + 1, :]
                    factors = jnp.exp(jnp.where(causal, spread, -jnp.inf))
                    weighed.append((products * factors).astype(BF16))
                inputs = xs[rows, lanes]
                zero = jnp.zeros_like(inputs)
                stacked = jnp.concatenate(
                    [jnp.where(low_half, inputs, zero), jnp.where(low_half, zero, inputs)], axis=0
                )
                within = dot(jnp.concatenate(weighed, axis=1), stacked)
                opened = silu(gate[rows, lanes].astype(F32))
                ysg[rows, lanes] = (ysg[rows, lanes] + within) * opened
                ersg[rows, lanes] = pair_columns(grown, j, low_half) * opened

    whole_dec = pltpu.make_async_copy(dec_recv, dec_recv, dec_sems.at[1])
    whole_dec.wait()
    pltpu.make_async_copy(sl_recv, sl_recv, sl_sems.at[1]).wait()

    def scan_step(j, state):
        d = lax.rem(me - j + n_sp, n_sp)
        pf_src[j] = state.astype(BF16)
        return jnp.exp(dec_recv[d]) * state + sl_recv[d].astype(F32)

    lax.fori_loop(0, n_sp, scan_step, jnp.zeros((16, 128), F32))

    def send_prefix(d, carry):
        target = lax.rem(me + d, n_sp)
        remote(pf_src.at[target], pf_recv.at[me], pf_sems.at[0], pf_sems.at[1], sp=target).start()
        return carry

    own_prefix = pltpu.make_async_copy(pf_src.at[me], pf_recv.at[me], pf_sems.at[1])
    own_prefix.start()
    lax.fori_loop(1, n_sp, send_prefix, 0)
    pltpu.make_async_copy(pf_recv, pf_recv, pf_sems.at[1]).wait()

    incoming = jnp.concatenate(
        [
            jnp.concatenate([pf_recv[pairs * i + j] for j in range(pairs)], axis=1)
            for i in range(STATE_WIDTH // 16)
        ],
        axis=0,
    ).astype(F32)
    for k in range(n_blocks):
        rows = slice(BLOCK * k, BLOCK * (k + 1))
        for g in range(groups):
            lanes = slice(group_width * g, group_width * (g + 1))
            carried = dot(cc[rows, 128 * g : 128 * (g + 1)], incoming[:, lanes].astype(BF16))
            gated = ysg[rows, lanes] + carried * ersg[rows, lanes]
            power = jnp.mean(gated * gated, axis=-1, keepdims=True)
            rows_out[rows, lanes] = (
                gated * lax.rsqrt(power + EPS) * gns[:, lanes].astype(F32)
            ).astype(BF16)
        if k + 1 < n_blocks:
            incoming = keep[k] * incoming + added[k]

    part = length // n_tp
    copies = []
    for d in (2, 1, 3, 0):
        target = lax.rem(col + d, n_tp)
        start = pl.multiple_of(target * part, part)
        for q in range(4):
            lanes = slice(512 * q, 512 * (q + 1))
            partial[pl.ds(start, part), lanes] = dot(
                rows_out[pl.ds(start, part), :], wout[:, lanes]
            ).astype(BF16)
        if d:
            copy = remote(
                partial.at[pl.ds(start, part)],
                arrived.at[d - 1],
                tp_sems.at[0, d - 1],
                tp_sems.at[1, d - 1],
                tp=target,
            )
            copy.start()
            copies.append(copy)
    for copy in copies:
        copy.wait()
    own = pl.multiple_of(col * part, part)
    mixed = partial[pl.ds(own, part), :].astype(F32)
    for d in range(n_tp - 1):
        mixed = mixed + arrived[d].astype(F32)
    mid[...] = layer_norm(ALPHA * resid[...].astype(F32) + mixed, n1s[...], n1b[...]).astype(BF16)

    def wait_sent(src, sems):
        remote(src, src, sems.at[0], sems.at[1], sp=after).wait_send()

    wait_sent(dec_recv.at[pl.ds(0, n_sp - 1)], dec_sems)
    wait_sent(sl_src.at[pl.ds(0, n_sp - 1)], sl_sems)
    wait_sent(pf_src.at[pl.ds(0, n_sp - 1)], pf_sems)


def expert_kernel(
    n_sp,
    cap,
    mid,
    routes,
    weights,
    wg,
    wu,
    wd,
    n2s,
    n2b,
    out,
    outgoing,
    received,
    answers,
    returned,
    tokens,
    hidden,
    wg_v,
    wu_v,
    wd_v,
    w_sems,
    there,
    back,
):
    me = lax.axis_index("sp")
    n_rows, width = mid.shape
    slots = n_sp * cap
    chunks = width // 128
    n_tp = wg.shape[0]
    loads = [
        pltpu.make_async_copy(src, dst, w_sems.at[i])
        for i, (src, dst) in enumerate(((wg, wg_v), (wu, wu_v), (wd, wd_v)))
    ]
    for load in loads:
        load.start()

    distance = routes[...] - me
    distance = jnp.where(distance < 0, distance + n_sp, distance)
    expert_id = lax.broadcasted_iota(jnp.int32, (n_rows, n_sp), 1)
    hits = [(expert_id == distance[:, k : k + 1]).astype(F32) for k in range(2)]
    r_id = lax.broadcasted_iota(jnp.int32, (n_rows, n_rows), 0)
    s_id = lax.broadcasted_iota(jnp.int32, (n_rows, n_rows), 1)
    before = dot((s_id < r_id).astype(BF16), (hits[0] + hits[1]).astype(BF16))
    slot_id = lax.broadcasted_iota(jnp.int32, (n_rows, slots), 1)
    at_slot = []
    for k in range(2):
        rank = jnp.sum(before * hits[k], axis=1, keepdims=True).astype(jnp.int32)
        at_slot.append(slot_id == distance[:, k : k + 1] * cap + rank)
    chosen = (at_slot[0] | at_slot[1]).astype(F32).astype(BF16)
    for q in range(4):
        lanes = slice(512 * q, 512 * (q + 1))
        piece = dot(chosen, mid[:, lanes], ((0,), (0,))).astype(BF16)
        outgoing[:, 4 * q : 4 * (q + 1), :] = piece.reshape(slots, 4, 128)

    def send_tokens(d, carry):
        target = lax.rem(me + d, n_sp)
        span = pl.ds(cap * d, cap)
        remote(outgoing.at[span], received.at[span], there.at[0], there.at[1], sp=target).start()
        return carry

    own = pltpu.make_async_copy(outgoing.at[pl.ds(0, cap)], received.at[pl.ds(0, cap)], there.at[1])
    own.start()
    lax.fori_loop(1, n_sp, send_tokens, 0)
    for load in loads:
        load.wait()
    pltpu.make_async_copy(received, received, there.at[1]).wait()

    tokens[...] = received[...].reshape(slots, width)

    def hidden_part(j, carry):
        opened = dot(tokens[...], wg_v[j])
        upward = dot(tokens[...], wu_v[j])
        hidden[j] = (silu(opened) * upward).astype(BF16)
        return carry

    lax.fori_loop(0, n_tp, hidden_part, 0)
    for q in range(width // 256):
        rows = slice(256 * q, 256 * (q + 1))
        total = dot(hidden[0], wd_v[0, rows, :], ((1,), (1,)))
        for j in range(1, n_tp):
            total = total + dot(hidden[j], wd_v[j, rows, :], ((1,), (1,)))
        answers[:, 2 * q : 2 * q + 2, :] = total.astype(BF16).reshape(slots, 2, 128)

    def send_answers(d, carry):
        target = lax.rem(me - d + n_sp, n_sp)
        span = pl.ds(cap * d, cap)
        remote(answers.at[span], returned.at[span], back.at[0], back.at[1], sp=target).start()
        return carry

    own = pltpu.make_async_copy(answers.at[pl.ds(0, cap)], returned.at[pl.ds(0, cap)], back.at[1])
    own.start()
    lax.fori_loop(1, n_sp, send_answers, 0)
    share = jnp.where(at_slot[0], weights[:, 0:1], 0.0) + jnp.where(at_slot[1], weights[:, 1:2], 0.0)
    coarse = share.astype(BF16)
    fine = (share - coarse.astype(F32)).astype(BF16)
    pltpu.make_async_copy(returned, returned, back.at[1]).wait()
    tokens[...] = returned[...].reshape(slots, width)
    ffn = dot(coarse, tokens[...]) + dot(fine, tokens[...])
    out[...] = layer_norm(ALPHA * mid[...].astype(F32) + ffn, n2s[...], n2b[...]).astype(BF16)

    rest = pl.ds(cap, slots - cap)
    for sems in (there, back):
        remote(
            outgoing.at[rest], received.at[rest], sems.at[0], sems.at[1], sp=lax.rem(me + 1, n_sp)
        ).wait_send()


def shards(n_sp, n_tp, *arguments):
    (
        head_input_values,
        group_input_vectors,
        group_readout_vectors,
        output_gate_values,
        step_size_logits,
        extra_log_decay,
        head_input_filter,
        input_vector_filter,
        readout_vector_filter,
        step_size_bias,
        head_rate_logarithm,
        direct_path_weight,
        group_norm_scale,
        mixer_output_weight,
        residual,
        first_norm_scale,
        first_norm_bias,
        routes,
        routing_weight,
        expert_gate_weight,
        expert_up_weight,
        expert_down_weight,
        final_norm_scale,
        final_norm_bias,
    ) = arguments
    gathered = [
        lax.all_gather(w.reshape(w.shape[1:]), "tp")
        for w in (expert_gate_weight, expert_up_weight, expert_down_weight)
    ]
    length, width = head_input_values.shape
    state_lanes = group_input_vectors.shape[1]
    rows_here, features = residual.shape
    n_blocks = length // BLOCK
    pairs = width // 128
    slices = (n_sp, 16, 128)
    vmem = pl.BlockSpec(memory_space=pltpu.VMEM)
    anywhere = pl.BlockSpec(memory_space=pl.ANY)
    dma = pltpu.SemaphoreType.DMA
    middle = pl.pallas_call(
        functools.partial(mixer_kernel, n_sp, n_tp),
        out_shape=jax.ShapeDtypeStruct((rows_here, features), BF16),
        in_specs=[vmem] * 17,
        out_specs=vmem,
        scratch_shapes=[
            pltpu.VMEM((8, width), BF16),
            pltpu.VMEM((8, state_lanes), BF16),
            pltpu.VMEM((8, state_lanes), BF16),
            pltpu.VMEM((length + 8, width), F32),
            pltpu.VMEM((length + 8, state_lanes), F32),
            pltpu.VMEM((length + 8, state_lanes), F32),
            pltpu.VMEM((pairs, 1, 128), F32),
            pltpu.VMEM((n_sp, 1, 128), F32),
            pltpu.VMEM(slices, BF16),
            pltpu.VMEM(slices, BF16),
            pltpu.VMEM(slices, BF16),
            pltpu.VMEM(slices, BF16),
            pltpu.VMEM((length, width), BF16),
            pltpu.VMEM((length, width), BF16),
            pltpu.VMEM((length, state_lanes), BF16),
            pltpu.VMEM((length, state_lanes), BF16),
            pltpu.VMEM((length, width), F32),
            pltpu.VMEM((length, width), F32),
            pltpu.VMEM((n_blocks, STATE_WIDTH, width), F32),
            pltpu.VMEM((length, width), BF16),
            pltpu.VMEM((length, features), BF16),
            pltpu.VMEM((n_tp - 1, rows_here, features), BF16),
            dma((2, 3)),
            dma((2,)),
            dma((2,)),
            dma((2,)),
            dma((2, n_tp - 1)),
        ],
        compiler_params=pltpu.CompilerParams(vmem_limit_bytes=VMEM_LIMIT, has_side_effects=True),
        cost_estimate=pl.CostEstimate(
            flops=40_000_000_000, bytes_accessed=10_000_000, transcendentals=0
        ),
        name="mixer",
    )(
        head_input_values,
        group_input_vectors,
        group_readout_vectors,
        output_gate_values,
        step_size_logits,
        extra_log_decay,
        head_input_filter,
        input_vector_filter,
        readout_vector_filter,
        step_size_bias.reshape(1, -1),
        head_rate_logarithm.reshape(1, -1),
        direct_path_weight.reshape(1, -1),
        group_norm_scale.reshape(1, -1),
        mixer_output_weight,
        residual,
        first_norm_scale.reshape(1, -1),
        first_norm_bias.reshape(1, -1),
    )
    experts = n_sp * expert_gate_weight.shape[0]
    cap = max(2, rows_here * routes.shape[1] * 5 // (3 * experts))
    slots = n_sp * cap
    tiles = (slots, features // 128, 128)
    part = expert_gate_weight.shape[2]
    return pl.pallas_call(
        functools.partial(expert_kernel, n_sp, cap),
        out_shape=jax.ShapeDtypeStruct((rows_here, features), BF16),
        in_specs=[vmem] * 3 + [anywhere] * 3 + [vmem] * 2,
        out_specs=vmem,
        scratch_shapes=[
            pltpu.VMEM(tiles, BF16),
            pltpu.VMEM(tiles, BF16),
            pltpu.VMEM(tiles, BF16),
            pltpu.VMEM(tiles, BF16),
            pltpu.VMEM((slots, features), BF16),
            pltpu.VMEM((n_tp, slots, part), BF16),
            pltpu.VMEM((n_tp, features, part), BF16),
            pltpu.VMEM((n_tp, features, part), BF16),
            pltpu.VMEM((n_tp, features, part), BF16),
            dma((3,)),
            dma((2,)),
            dma((2,)),
        ],
        compiler_params=pltpu.CompilerParams(vmem_limit_bytes=VMEM_LIMIT, has_side_effects=True),
        cost_estimate=pl.CostEstimate(
            flops=40_000_000_000, bytes_accessed=10_000_000, transcendentals=0
        ),
        name="experts",
    )(
        middle,
        routes,
        routing_weight,
        *gathered,
        final_norm_scale.reshape(1, -1),
        final_norm_bias.reshape(1, -1),
    )


def solution(mesh):
    every = P(("sp", "tp"), None)
    placed = (
        *([P("sp", "tp")] * 6),
        *([P(None, "tp")] * 3),
        *([P("tp")] * 4),
        P("tp", None),
        every,
        P(),
        P(),
        every,
        every,
        *([P("sp", None, "tp")] * 3),
        P(),
        P(),
    )
    return jax.shard_map(
        functools.partial(shards, mesh.shape["sp"], mesh.shape["tp"]),
        mesh=mesh,
        in_specs=placed,
        out_specs=every,
        check_vma=False,
    )
```

time: 399 us -> 272 us (0.68)
  Pallas kernels: 0 us -> 156 us
  blocking collectives: 89.3 us -> 0 us
  local copies, waits for them, and re-layouts: 86.9 us -> 8.93 us
  waiting for transfers between devices: 134 us -> 92 us
  matrix products: 25.7 us -> 0 us
  starting transfers between devices: 24 us -> 0.08 us
  other arithmetic: 22.4 us -> 0 us
    pallas_call x0 -> x2, Pallas kernels: none -> 156 us  [the longest x1 86.5 us: shards(): pl.pallas_call(functools.partial(expert_kernel, n_sp, cap), out_shape=jax...]
    all_to_all x2 -> x0, waiting for transfers between devices: 83.5 us -> none  [the longest x1 49.5 us: shards(): lax.all_to_all(answers, SP, split_axis=0, concat_axis=0, tiled=True)]
    all_to_all x1 -> x0, blocking collectives: 63.3 us -> none  [shards(): lax.all_to_all(outgoing, SP, split_axis=0, concat_axis=0, tiled=True)]
    dynamic_update_slice x3 -> x0, local copies, waits for them, and re-layouts: 41.5 us -> none  [shards(): lax.scan(block_pass, start_state, (step_scaled_inputs.reshape(block_list,...]
    all_gather x3, waiting for transfers between devices: 50.8 us -> 89.9 us  [shards(): lax.all_gather(w.reshape(w.shape[1:]), 'tp')]
    all_gather x4 -> x0, blocking collectives: 26 us -> none  [prefix_by_axis(): lax.all_gather(part.astype(kind), axis)]
    dot_general x16 -> x0, matrix products: 25.7 us -> none  [the longest x1 8.13 us: expert_output(): jnp.einsum('senf,edf->send', hidden, weight_down, preferred_element_type=...]
    all_to_all x2 -> x0, starting transfers between devices: 13.8 us -> none  [the longest x1 9.87 us: shards(): lax.all_to_all(answers, SP, split_axis=0, concat_axis=0, tiled=True)]
  transfers between devices with their start and end apart: 8 -> 3, of which waited for: 5 -> 2; matrix products, arithmetic and copies ran while one was open for 11% -> 3% of each run, Pallas kernels for 0% -> 26%
where the time goes in v1:
time: 272 us; the launch traced here: 270 us
  Pallas kernels  156 us (57%)
  waiting for transfers between devices  92 us (34%)
  between operations  13.1 us (5%)
  local copies, waits for them, and re-layouts  8.93 us (3%)
    all_gather x3, waiting for transfers between devices, shards(): lax.all_gather(w.reshape(w.shape[1:]), 'tp')  89.9 us
    pallas_call x1, Pallas kernels, shards(): pl.pallas_call(functools.partial(expert_kernel, n_sp, cap), out_shape=jax...  86.5 us
    pallas_call x1, Pallas kernels, shards(): pl.pallas_call(functools.partial(mixer_kernel, n_sp, n_tp), out_shape=jax...  69.7 us
    unnamed x5, local copies, waits for them, and re-layouts  7.65 us
  transfers between devices with their start and end apart: 3, of which 2 were waited for; matrix products, arithmetic and copies ran while one was open for 3% of the time, Pallas kernels for 26%

profile of v1, /device:TPU:1, one launch (start us, length us, event | category | flops | bytes accessed | tf_op | source)
XLA Modules:
  0.0 270.4 jit_solution(13217475973560814344)
XLA Ops:
  6.5 0.0 all-gather.4.cloned.1.call-start
  6.5 0.7 all-gather.4.cloned.1.call-update
  7.3 0.0 all-gather.6.cloned.1.call-start
  7.3 0.7 all-gather.6.cloned.1.call-update
  8.0 0.0 all-gather.8.cloned.1.call-start
  8.1 0.7 all-gather.8.cloned.1.call-update
  8.7 1.5 copy.29.logits
  10.3 1.5 copy.30.extra
  11.8 1.3 reshape.27.gns
  13.1 1.4 copy.31.routes
  14.5 1.4 copy.32.weights
  15.9 69.7 %mixer.1.mid = bf16[96,2048]{1,0:T(8,128)(2,1)} custom-call(bf16[384,1024]{1,0:T(8,128)(2,1)} %x.1, bf16[384,256]{1,0:T(8,128)(2,1)} %b.1, bf16[384,256]{1,0:T(8,128)(2,1)} %c.1, bf16[384,1024]{1,0:T(8,128)(2,1)} %gate.1, f32[384,16]{1,0:T(8,128)} %copy.29.logits, f32[384,16]{1,0:T(8,128)} %copy.30.extra, bf16[4,1024]{1,0:T(4,128)(2,1)} %fx.1, ...), custom_call_target="tpu_custom_call" | custom-call | flops 40000000000 | bytes 10000000 | tf_op jit(solution)/shard_map/mixer/pallas_call | solution.py:475
  85.7 0.0 all-gather.4.cloned.1.call-done.wg
  85.7 37.0 %all-gather.6.cloned.1.call-done.wu = bf16[4,2048,256]{2,1,0:T(8,128)(2,1)} async-done(((bf16[1,2048,256]{2,1,0:T(8,128)(2,1)}), bf16[4,2048,256]{2,1,0:T(8,128)(2,1)}) %all-gather.6.cloned.1.call-update) | async-done | bytes 4194320 | tf_op jit(solution)/shard_map/all_gather | solution.py:463
  122.7 53.0 %all-gather.8.cloned.1.call-done.wd = bf16[4,2048,256]{2,1,0:T(8,128)(2,1)} async-done(((bf16[1,2048,256]{2,1,0:T(8,128)(2,1)}), bf16[4,2048,256]{2,1,0:T(8,128)(2,1)}) %all-gather.8.cloned.1.call-update) | async-done | bytes 4194320 | tf_op jit(solution)/shard_map/all_gather | solution.py:463
  175.6 86.5 %experts.1 = bf16[96,2048]{1,0:T(8,128)(2,1)} custom-call(bf16[96,2048]{1,0:T(8,128)(2,1)} %mixer.1.mid, s32[96,2]{1,0:T(8,128)} %copy.31.routes, f32[96,2]{1,0:T(8,128)} %copy.32.weights, bf16[4,2048,256]{2,1,0:T(8,128)(2,1)} %all-gather.4.cloned.1.call-done.wg, bf16[4,2048,256]{2,1,0:T(8,128)(2,1)} %all-gather.6.cloned.1.call-done.wu, ...), custom_call_target="tpu_custom_call" | custom-call | flops 40000000000 | bytes 10000000 | tf_op jit(solution)/shard_map/experts/pallas_call | solution.py:538
  262.1 1.8 copy.34
Async XLA Ops:
  6.5 79.1 %all-gather.4.cloned.1.call-start = ((), (), s32[]{:S(2)}) async-start(), calls=%async_computation | async-start | bytes 5242880 | tf_op jit(solution)/shard_map/all_gather | solution.py:463
  7.3 115.4 %all-gather.6.cloned.1.call-start = ((), (), s32[]{:S(2)}) async-start(), calls=%async_computation.1 | async-start | bytes 5242880 | tf_op jit(solution)/shard_map/all_gather | solution.py:463
  8.0 167.6 %all-gather.8.cloned.1.call-start = ((), (), s32[]{:S(2)}) async-start(), calls=%async_computation.2 | async-start | bytes 5242880 | tf_op jit(solution)/shard_map/all_gather | solution.py:463
Sparse Core Ops, SparseCore 0:
  9.1 54.3 all-gather.3
  65.3 57.2 all-gather.5
  124.5 51.0 all-gather.7

commit v2 on v1

--- a/solution.py
+++ b/solution.py
@@ -57,9 +57,10 @@
     return jnp.where(low_half[:rows], first, second)
 
 
-def mixer_kernel(
+def fused_kernel(
     n_sp,
     n_tp,
+    cap,
     x,
     b,
     c,
@@ -73,11 +74,18 @@
     rate,
     direct,
     gns,
-    wout,
     resid,
     n1s,
     n1b,
-    mid,
+    routes,
+    weights,
+    n2s,
+    n2b,
+    wout_h,
+    wg,
+    wu,
+    wd,
+    out,
     tail_x,
     tail_b,
     tail_c,
@@ -100,14 +108,73 @@
     rows_out,
     partial,
     arrived,
+    wout,
+    mid,
+    outgoing,
+    received,
+    answers,
+    returned,
+    tokens,
+    hidden,
+    wg_v,
+    wu_v,
+    wd_v,
     tail_sems,
     dec_sems,
     sl_sems,
     pf_sems,
     tp_sems,
+    wout_sem,
+    w_first,
+    w_recv,
+    w_relay,
+    w_side,
+    there,
+    back,
 ):
     me = lax.axis_index("sp")
     col = lax.axis_index("tp")
+    core = lax.rem(me, 2)
+    beside = col + 1 - 2 * lax.rem(col, 2)
+    across_x = n_tp - 1 - col
+    sibling = me + 1 - 2 * core
+    home = lax.div(col, 2) == core
+    moves = tuple(enumerate(((wg, wg_v), (wu, wu_v), (wd, wd_v))))
+
+    def arrival(m, place):
+        block = moves[m][1][1].at[place]
+        return pltpu.make_async_copy(block, block, w_recv.at[place, m])
+
+    def first_hop(m):
+        src, dst = moves[m][1]
+        target = jnp.where(home, beside, across_x)
+        return remote(src.at[0], dst.at[col], w_first.at[m], w_recv.at[col, m], tp=target)
+
+    def relay(m):
+        block = moves[m][1][1].at[across_x]
+        return remote(block, block, w_relay.at[m], w_recv.at[across_x, m], tp=beside)
+
+    def sideways(m, place, src=None):
+        block = moves[m][1][1].at[place]
+        return remote(
+            block if src is None else src,
+            block,
+            w_side.at[place, m],
+            w_recv.at[place, m],
+            sp=sibling,
+        )
+
+    for m in range(3):
+        first_hop(m).start()
+
+    @pl.when(home)
+    def _():
+        for m in range(3):
+            src, dst = moves[m][1]
+            pltpu.make_async_copy(src.at[0], dst.at[col], w_recv.at[col, m]).start()
+            sideways(m, col, src.at[0]).start()
+
+    pltpu.make_async_copy(wout_h, wout, wout_sem).start()
     length, width = x.shape
     n_blocks = length // BLOCK
     pairs = width // 128
@@ -128,9 +195,9 @@
     causal = row_id >= lane_id
     lower = causal.astype(F32)
 
-    raw = logits[...] + bias[...]
+    raw = logits[...].T + bias[...]
     steps = jnp.maximum(raw, 0.0) + jnp.log(1.0 + jnp.exp(-jnp.abs(raw)))
-    decay = -steps * jnp.exp(rate[...]) + extra[...]
+    decay = -steps * jnp.exp(rate[...]) + extra[...].T
     running = [
         dot(lower, decay[BLOCK * k : BLOCK * (k + 1)], precision=lax.Precision.HIGHEST)
         for k in range(n_blocks)
@@ -268,6 +335,7 @@
     lax.fori_loop(1, n_sp, send_prefix, 0)
     pltpu.make_async_copy(pf_recv, pf_recv, pf_sems.at[1]).wait()
 
+    gain = gns[...].astype(F32).reshape(1, width)
     incoming = jnp.concatenate(
         [
             jnp.concatenate([pf_recv[pairs * i + j] for j in range(pairs)], axis=1)
@@ -283,11 +351,12 @@
             gated = ysg[rows, lanes] + carried * ersg[rows, lanes]
             power = jnp.mean(gated * gated, axis=-1, keepdims=True)
             rows_out[rows, lanes] = (
-                gated * lax.rsqrt(power + EPS) * gns[:, lanes].astype(F32)
+                gated * lax.rsqrt(power + EPS) * gain[:, lanes]
             ).astype(BF16)
         if k + 1 < n_blocks:
             incoming = keep[k] * incoming + added[k]
 
+    pltpu.make_async_copy(wout_h, wout, wout_sem).wait()
     part = length // n_tp
     copies = []
     for d in (2, 1, 3, 0):
@@ -308,6 +377,16 @@
             )
             copy.start()
             copies.append(copy)
+
+    @pl.when(home)
+    def _():
+        for m in range(3):
+            arrival(m, across_x).wait()
+            relay(m).start()
+            sideways(m, across_x).start()
+            arrival(m, beside).wait()
+            sideways(m, beside).start()
+
     for copy in copies:
         copy.wait()
     own = pl.multiple_of(col * part, part)
@@ -316,53 +395,15 @@
         mixed = mixed + arrived[d].astype(F32)
     mid[...] = layer_norm(ALPHA * resid[...].astype(F32) + mixed, n1s[...], n1b[...]).astype(BF16)
 
-    def wait_sent(src, sems):
-        remote(src, src, sems.at[0], sems.at[1], sp=after).wait_send()
-
-    wait_sent(dec_recv.at[pl.ds(0, n_sp - 1)], dec_sems)
-    wait_sent(sl_src.at[pl.ds(0, n_sp - 1)], sl_sems)
-    wait_sent(pf_src.at[pl.ds(0, n_sp - 1)], pf_sems)
-
-
-def expert_kernel(
-    n_sp,
-    cap,
-    mid,
-    routes,
-    weights,
-    wg,
-    wu,
-    wd,
-    n2s,
-    n2b,
-    out,
-    outgoing,
-    received,
-    answers,
-    returned,
-    tokens,
-    hidden,
-    wg_v,
-    wu_v,
-    wd_v,
-    w_sems,
-    there,
-    back,
-):
-    me = lax.axis_index("sp")
-    n_rows, width = mid.shape
+    n_rows, features = mid.shape
     slots = n_sp * cap
-    chunks = width // 128
-    n_tp = wg.shape[0]
-    loads = [
-        pltpu.make_async_copy(src, dst, w_sems.at[i])
-        for i, (src, dst) in enumerate(((wg, wg_v), (wu, wu_v), (wd, wd_v)))
-    ]
-    for load in loads:
-        load.start()
-
-    distance = routes[...] - me
-    distance = jnp.where(distance < 0, distance + n_sp, distance)
+    named = routes[...].astype(F32).T.astype(jnp.int32)
+    chip = lax.div(me, 2)
+    n_chips = n_sp // 2
+    distance = lax.shift_right_logical(named, 1) - chip
+    distance = jnp.where(distance < 0, distance + n_chips, distance)
+    distance = 2 * distance + jnp.where((named & 1) == lax.div(col, 2), 0, 1)
+    shares = weights[...].T
     expert_id = lax.broadcasted_iota(jnp.int32, (n_rows, n_sp), 1)
     hits = [(expert_id == distance[:, k : k + 1]).astype(F32) for k in range(2)]
     r_id = lax.broadcasted_iota(jnp.int32, (n_rows, n_rows), 0)
@@ -379,20 +420,38 @@
         piece = dot(chosen, mid[:, lanes], ((0,), (0,))).astype(BF16)
         outgoing[:, 4 * q : 4 * (q + 1), :] = piece.reshape(slots, 4, 128)
 
+    def plane(d):
+        return col + lax.rem(d, 2) * (across_x - col)
+
     def send_tokens(d, carry):
-        target = lax.rem(me + d, n_sp)
+        target = 2 * lax.rem(chip + lax.div(d, 2), n_chips) + core
         span = pl.ds(cap * d, cap)
-        remote(outgoing.at[span], received.at[span], there.at[0], there.at[1], sp=target).start()
+        remote(
+            outgoing.at[span], received.at[span], there.at[0], there.at[1], sp=target, tp=plane(d)
+        ).start()
         return carry
 
     own = pltpu.make_async_copy(outgoing.at[pl.ds(0, cap)], received.at[pl.ds(0, cap)], there.at[1])
     own.start()
     lax.fori_loop(1, n_sp, send_tokens, 0)
-    for load in loads:
-        load.wait()
+
+    @pl.when(home)
+    def _():
+        for m in range(3):
+            last = n_tp - 1 - beside
+            arrival(m, last).wait()
+            sideways(m, last).start()
+            arrival(m, col).wait()
+
+    @pl.when(jnp.logical_not(home))
+    def _():
+        for m in range(3):
+            for place in range(n_tp):
+                arrival(m, place).wait()
+
     pltpu.make_async_copy(received, received, there.at[1]).wait()
 
-    tokens[...] = received[...].reshape(slots, width)
+    tokens[...] = received[...].reshape(slots, features)
 
     def hidden_part(j, carry):
         opened = dot(tokens[...], wg_v[j])
@@ -401,7 +460,7 @@
         return carry
 
     lax.fori_loop(0, n_tp, hidden_part, 0)
-    for q in range(width // 256):
+    for q in range(features // 256):
         rows = slice(256 * q, 256 * (q + 1))
         total = dot(hidden[0], wd_v[0, rows, :], ((1,), (1,)))
         for j in range(1, n_tp):
@@ -409,27 +468,43 @@
         answers[:, 2 * q : 2 * q + 2, :] = total.astype(BF16).reshape(slots, 2, 128)
 
     def send_answers(d, carry):
-        target = lax.rem(me - d + n_sp, n_sp)
+        target = 2 * lax.rem(chip - lax.div(d, 2) + n_chips, n_chips) + core
         span = pl.ds(cap * d, cap)
-        remote(answers.at[span], returned.at[span], back.at[0], back.at[1], sp=target).start()
+        remote(
+            answers.at[span], returned.at[span], back.at[0], back.at[1], sp=target, tp=plane(d)
+        ).start()
         return carry
 
     own = pltpu.make_async_copy(answers.at[pl.ds(0, cap)], returned.at[pl.ds(0, cap)], back.at[1])
     own.start()
     lax.fori_loop(1, n_sp, send_answers, 0)
-    share = jnp.where(at_slot[0], weights[:, 0:1], 0.0) + jnp.where(at_slot[1], weights[:, 1:2], 0.0)
+    share = jnp.where(at_slot[0], shares[:, 0:1], 0.0) + jnp.where(at_slot[1], shares[:, 1:2], 0.0)
     coarse = share.astype(BF16)
     fine = (share - coarse.astype(F32)).astype(BF16)
     pltpu.make_async_copy(returned, returned, back.at[1]).wait()
-    tokens[...] = returned[...].reshape(slots, width)
+    tokens[...] = returned[...].reshape(slots, features)
     ffn = dot(coarse, tokens[...]) + dot(fine, tokens[...])
     out[...] = layer_norm(ALPHA * mid[...].astype(F32) + ffn, n2s[...], n2b[...]).astype(BF16)
 
+    def wait_sent(src, sems):
+        remote(src, src, sems.at[0], sems.at[1], sp=after).wait_send()
+
+    wait_sent(dec_recv.at[pl.ds(0, n_sp - 1)], dec_sems)
+    wait_sent(sl_src.at[pl.ds(0, n_sp - 1)], sl_sems)
+    wait_sent(pf_src.at[pl.ds(0, n_sp - 1)], pf_sems)
+
     rest = pl.ds(cap, slots - cap)
     for sems in (there, back):
-        remote(
-            outgoing.at[rest], received.at[rest], sems.at[0], sems.at[1], sp=lax.rem(me + 1, n_sp)
-        ).wait_send()
+        wait_sent(outgoing.at[rest], sems)
+    for m in range(3):
+        first_hop(m).wait_send()
+
+    @pl.when(home)
+    def _():
+        for m in range(3):
+            relay(m).wait_send()
+            for place in range(n_tp):
+                sideways(m, place).wait_send()
 
 
 def shards(n_sp, n_tp, *arguments):
@@ -459,10 +534,6 @@
         final_norm_scale,
         final_norm_bias,
     ) = arguments
-    gathered = [
-        lax.all_gather(w.reshape(w.shape[1:]), "tp")
-        for w in (expert_gate_weight, expert_up_weight, expert_down_weight)
-    ]
     length, width = head_input_values.shape
     state_lanes = group_input_vectors.shape[1]
     rows_here, features = residual.shape
@@ -472,10 +543,15 @@
     vmem = pl.BlockSpec(memory_space=pltpu.VMEM)
     anywhere = pl.BlockSpec(memory_space=pl.ANY)
     dma = pltpu.SemaphoreType.DMA
-    middle = pl.pallas_call(
-        functools.partial(mixer_kernel, n_sp, n_tp),
+    experts = n_sp * expert_gate_weight.shape[0]
+    cap = max(2, rows_here * routes.shape[1] * 5 // (3 * experts))
+    slots = n_sp * cap
+    tiles = (slots, features // 128, 128)
+    part = expert_gate_weight.shape[2]
+    return pl.pallas_call(
+        functools.partial(fused_kernel, n_sp, n_tp, cap),
         out_shape=jax.ShapeDtypeStruct((rows_here, features), BF16),
-        in_specs=[vmem] * 17,
+        in_specs=[vmem] * 20 + [anywhere] * 4,
         out_specs=vmem,
         scratch_shapes=[
             pltpu.VMEM((8, width), BF16),
@@ -500,47 +576,8 @@
             pltpu.VMEM((length, width), BF16),
             pltpu.VMEM((length, features), BF16),
             pltpu.VMEM((n_tp - 1, rows_here, features), BF16),
-            dma((2, 3)),
-            dma((2,)),
-            dma((2,)),
-            dma((2,)),
-            dma((2, n_tp - 1)),
-        ],
-        compiler_params=pltpu.CompilerParams(vmem_limit_bytes=VMEM_LIMIT, has_side_effects=True),
-        cost_estimate=pl.CostEstimate(
-            flops=40_000_000_000, bytes_accessed=10_000_000, transcendentals=0
-        ),
-        name="mixer",
-    )(
-        head_input_values,
-        group_input_vectors,
-        group_readout_vectors,
-        output_gate_values,
-        step_size_logits,
-        extra_log_decay,
-        head_input_filter,
-        input_vector_filter,
-        readout_vector_filter,
-        step_size_bias.reshape(1, -1),
-        head_rate_logarithm.reshape(1, -1),
-        direct_path_weight.reshape(1, -1),
-        group_norm_scale.reshape(1, -1),
-        mixer_output_weight,
-        residual,
-        first_norm_scale.reshape(1, -1),
-        first_norm_bias.reshape(1, -1),
-    )
-    experts = n_sp * expert_gate_weight.shape[0]
-    cap = max(2, rows_here * routes.shape[1] * 5 // (3 * experts))
-    slots = n_sp * cap
-    tiles = (slots, features // 128, 128)
-    part = expert_gate_weight.shape[2]
-    return pl.pallas_call(
-        functools.partial(expert_kernel, n_sp, cap),
-        out_shape=jax.ShapeDtypeStruct((rows_here, features), BF16),
-        in_specs=[vmem] * 3 + [anywhere] * 3 + [vmem] * 2,
-        out_specs=vmem,
-        scratch_shapes=[
+            pltpu.VMEM((width, features), BF16),
+            pltpu.VMEM((rows_here, features), BF16),
             pltpu.VMEM(tiles, BF16),
             pltpu.VMEM(tiles, BF16),
             pltpu.VMEM(tiles, BF16),
@@ -550,22 +587,46 @@
             pltpu.VMEM((n_tp, features, part), BF16),
             pltpu.VMEM((n_tp, features, part), BF16),
             pltpu.VMEM((n_tp, features, part), BF16),
+            dma((2, 3)),
+            dma((2,)),
+            dma((2,)),
+            dma((2,)),
+            dma((2, n_tp - 1)),
+            dma(()),
             dma((3,)),
+            dma((n_tp, 3)),
+            dma((3,)),
+            dma((n_tp, 3)),
             dma((2,)),
             dma((2,)),
         ],
         compiler_params=pltpu.CompilerParams(vmem_limit_bytes=VMEM_LIMIT, has_side_effects=True),
-        cost_estimate=pl.CostEstimate(
-            flops=40_000_000_000, bytes_accessed=10_000_000, transcendentals=0
-        ),
-        name="experts",
+        name="fused",
     )(
-        middle,
-        routes,
-        routing_weight,
-        *gathered,
+        head_input_values,
+        group_input_vectors,
+        group_readout_vectors,
+        output_gate_values,
+        step_size_logits.T,
+        extra_log_decay.T,
+        head_input_filter,
+        input_vector_filter,
+        readout_vector_filter,
+        step_size_bias.reshape(1, -1),
+        head_rate_logarithm.reshape(1, -1),
+        direct_path_weight.reshape(1, -1),
+        group_norm_scale,
+        residual,
+        first_norm_scale.reshape(1, -1),
+        first_norm_bias.reshape(1, -1),
+        routes.T,
+        routing_weight.T,
         final_norm_scale.reshape(1, -1),
         final_norm_bias.reshape(1, -1),
+        mixer_output_weight,
+        expert_gate_weight,
+        expert_up_weight,
+        expert_down_weight,
     )
 
 

time: 272 us -> 151 us (0.56)
  waiting for transfers between devices: 92 us -> 0 us
  between operations: 13.1 us -> 0.01 us
  local copies, waits for them, and re-layouts: 8.93 us -> 1.77 us
  Pallas kernels: 156 us -> 149 us
    all_gather x3 -> x0, waiting for transfers between devices: 89.9 us -> none  [shards(): lax.all_gather(w.reshape(w.shape[1:]), 'tp')]
    pallas_call x2 -> x1, Pallas kernels: 156 us -> 149 us  [shards(): pl.pallas_call(functools.partial(fused_kernel, n_sp, n_tp, cap), out_shap...]
    unnamed x5 -> x1, local copies, waits for them, and re-layouts: 7.65 us -> 1.77 us
  transfers between devices with their start and end apart: 3 -> 0, of which waited for: 2 -> 0; matrix products, arithmetic and copies ran while one was open for 3% -> 0% of each run, Pallas kernels for 26% -> 0%
where the time goes in v2:
time: 151 us
  Pallas kernels  149 us (99%)
  local copies, waits for them, and re-layouts  1.77 us (1%)
    pallas_call x1, Pallas kernels, shards(): pl.pallas_call(functools.partial(fused_kernel, n_sp, n_tp, cap), out_shap...  149 us

profile of v2, /device:TPU:1, one launch (start us, length us, event | category | flops | bytes accessed | tf_op | source)
XLA Modules:
  0.0 150.7 jit_solution(16574344949417408772)
XLA Ops:
  0.0 148.9 %fused.1 = bf16[96,2048]{1,0:T(8,128)(2,1)} custom-call(bf16[384,1024]{1,0:T(8,128)(2,1)} %x.1, bf16[384,256]{1,0:T(8,128)(2,1)} %b.1, bf16[384,256]{1,0:T(8,128)(2,1)} %c.1, bf16[384,1024]{1,0:T(8,128)(2,1)} %gate.1, f32[16,384]{1,0:T(8,128)} %bitcast.11, f32[16,384]{1,0:T(8,128)} %bitcast.12, bf16[4,1024]{1,0:T(4,128)(2,1)} %fx.1, bf16[4,256]{1,0:T(4,128)(2,1)} %fb.1, ...), custom_call_target="tpu_custom_call" | custom-call | tf_op jit(solution)/shard_map/fused/pallas_call | solution.py:551
  148.9 1.8 %copy.26 = bf16[96,2048]{1,0:T(8,128)(2,1)} copy(bf16[96,2048]{1,0:T(8,128)(2,1)} %fused.1) | data formatting | bytes 786432

commit v3 on v2

v3 whole, which is shorter than its diff:
```python
import functools

import jax
import jax.numpy as jnp
from jax import lax
from jax.experimental import pallas as pl
from jax.experimental.pallas import tpu as pltpu
from jax.sharding import PartitionSpec as P

HEAD_DIM = 64
STATE_WIDTH = 128
BLOCK = 128
EPS = 1e-05
ALPHA = 8.0**0.25
F32 = jnp.float32
BF16 = jnp.bfloat16
VMEM_LIMIT = 62 * 1024 * 1024


def dot(a, b, dims=((1,), (0,)), precision=None):
    return lax.dot_general(
        a, b, (dims, ((), ())), preferred_element_type=F32, precision=precision
    )


def silu(v):
    return v * (1.0 / (1.0 + jnp.exp(-v)))


def layer_norm(values, gain_row, bias_row):
    mean_value = jnp.mean(values, axis=-1, keepdims=True)
    centred = values - mean_value
    spread = jnp.mean(centred * centred, axis=-1, keepdims=True)
    return centred * lax.rsqrt(spread + EPS) * gain_row + bias_row


def remote(src, dst, send, recv, sp=None, tp=None):
    target = {}
    if sp is not None:
        target["sp"] = sp
    if tp is not None:
        target["tp"] = tp
    return pltpu.make_async_remote_copy(
        src_ref=src,
        dst_ref=dst,
        send_sem=send,
        recv_sem=recv,
        device_id=target,
        device_id_type=pl.DeviceIdType.MESH,
    )


def pair_columns(values, pair, low_half):
    rows = values.shape[0]
    first = jnp.broadcast_to(values[:, 2 * pair : 2 * pair + 1], (rows, 128))
    second = jnp.broadcast_to(values[:, 2 * pair + 1 : 2 * pair + 2], (rows, 128))
    return jnp.where(low_half[:rows], first, second)


def fused_kernel(n_sp, n_tp, cap, *refs):
    hbm, out, refs = refs[:24], refs[24], refs[25:]
    loaded, refs = refs[:21], refs[21:]
    (x, b, c, gate, logits, extra, fx, fb, fc, bias, rate, direct, gns, resid) = loaded[:14]
    (n1s, n1b, routes, weights, n2s, n2b, wout) = loaded[14:]
    wg, wu, wd = hbm[21:]
    (
        tail_x,
        tail_b,
        tail_c,
        ext_x,
        ext_b,
        ext_c,
        dec_src,
        dec_recv,
        sl_src,
        sl_recv,
        pf_src,
        pf_recv,
        xs,
        xw,
        cb,
        cc,
        ysg,
        ersg,
        added,
        rows_out,
        partial,
        relayed,
        arrived,
        mid,
        outgoing,
        received,
        answers,
        returned,
        tokens,
        hidden,
        summed,
        wg_v,
        wu_v,
        wd_v,
        load_sems,
        tail_sems,
        dec_sems,
        sl_sems,
        pf_sems,
        tp_sems,
        w_first,
        w_recv,
        w_relay,
        w_side,
        there,
        back,
    ) = refs
    me = lax.axis_index("sp")
    col = lax.axis_index("tp")
    core = lax.rem(me, 2)
    chip = lax.div(me, 2)
    n_chips = n_sp // 2
    beside = col + 1 - 2 * lax.rem(col, 2)
    across_x = n_tp - 1 - col
    last_place = n_tp - 1 - beside
    sibling = me + 1 - 2 * core
    home = lax.div(col, 2) == core
    moves = tuple(enumerate(((wg, wg_v), (wu, wu_v), (wd, wd_v))))
    length, width = x.shape
    n_blocks = length // BLOCK
    pairs = width // 128
    groups = b.shape[1] // STATE_WIDTH
    group_width = width // groups
    n_rows, features = mid.shape
    slots = n_sp * cap

    loads = [
        pltpu.make_async_copy(hbm[i], loaded[i], load_sems.at[i]) for i in range(len(loaded))
    ]
    order = (4, 5, 9, 10, 0, 1, 6, 7, 11, 2, 8, 3, 12, 20, 13, 14, 15, 16, 17, 18, 19)
    for i in order:
        loads[i].start()
    barrier = pltpu.get_barrier_semaphore()

    def greet(sp, tp):
        pl.semaphore_signal(
            barrier, inc=1, device_id={"sp": sp, "tp": tp}, device_id_type=pl.DeviceIdType.MESH
        )

    def greet_column(d, carry):
        greet(lax.rem(me + d, n_sp), col)
        return carry

    def greet_plane(q, carry):
        greet(2 * lax.rem(chip + q, n_chips) + core, across_x)
        return carry

    lax.fori_loop(1, n_sp, greet_column, 0)
    lax.fori_loop(0, n_chips, greet_plane, 0)
    greet(me, beside)
    greet(me, last_place)

    def arrival(m, place):
        block = moves[m][1][1].at[place]
        return pltpu.make_async_copy(block, block, w_recv.at[place, m])

    def first_hop(m):
        src, dst = moves[m][1]
        target = jnp.where(home, beside, across_x)
        return remote(src.at[0], dst.at[col], w_first.at[m], w_recv.at[col, m], tp=target)

    def relay(m):
        block = moves[m][1][1].at[across_x]
        return remote(block, block, w_relay.at[m], w_recv.at[across_x, m], tp=beside)

    def sideways(m, place, src=None):
        block = moves[m][1][1].at[place]
        return remote(
            block if src is None else src,
            block,
            w_side.at[place, m],
            w_recv.at[place, m],
            sp=sibling,
        )

    low_half = lax.broadcasted_iota(jnp.int32, (BLOCK, 128), 1) < 64
    row_id = lax.broadcasted_iota(jnp.int32, (BLOCK, BLOCK), 0)
    lane_id = lax.broadcasted_iota(jnp.int32, (BLOCK, BLOCK), 1)
    causal = row_id >= lane_id
    lower = causal.astype(F32)

    for i in (4, 5, 9, 10):
        loads[i].wait()
    raw = logits[...].T + bias[...]
    steps = jnp.maximum(raw, 0.0) + jnp.log(1.0 + jnp.exp(-jnp.abs(raw)))
    decay = -steps * jnp.exp(rate[...]) + extra[...].T
    running = [
        dot(lower, decay[BLOCK * k : BLOCK * (k + 1)], precision=lax.Precision.HIGHEST)
        for k in range(n_blocks)
    ]
    totals = [r[BLOCK - 1 : BLOCK] for r in running]
    whole = functools.reduce(lambda p, q: p + q, totals)
    for j in range(pairs):
        dec_src[j] = pair_columns(whole, j, low_half)

    for i in (0, 1, 6, 7):
        loads[i].wait()
    ext_x[8:, :] = x[...].astype(F32)
    ext_b[8:, :] = b[...].astype(F32)

    def conv(ext, taps, k, j):
        lanes = slice(128 * j, 128 * (j + 1))
        total = None
        for i in range(4):
            start = BLOCK * k + 5 + i
            term = taps[i : i + 1, lanes].astype(F32) * ext[start : start + BLOCK, lanes]
            total = term if total is None else total + term
        return silu(total)

    def inputs_of_block(k):
        rows = slice(BLOCK * k, BLOCK * (k + 1))
        for g in range(groups):
            cb[rows, 128 * g : 128 * (g + 1)] = conv(ext_b, fb, k, g).astype(BF16)
        to_end = steps[rows] * jnp.exp(totals[k] - running[k])
        for j in range(pairs):
            lanes = slice(128 * j, 128 * (j + 1))
            value = conv(ext_x, fx, k, j)
            ysg[rows, lanes] = value
            xw[rows, lanes] = (value * pair_columns(to_end, j, low_half)).astype(BF16)
        for g in range(groups):
            lanes = slice(group_width * g, group_width * (g + 1))
            added[k, :, lanes] = dot(
                cb[rows, 128 * g : 128 * (g + 1)], xw[rows, lanes], ((0,), (0,))
            )

    for k in range(n_blocks - 1, 0, -1):
        inputs_of_block(k)

    loads[2].wait()
    pl.semaphore_wait(barrier, n_sp - 1 + n_chips + 2)
    after = lax.rem(me + 1, n_sp)
    tails = [
        remote(v.at[pl.ds(length - 8, 8)], t, tail_sems.at[0, i], tail_sems.at[1, i], sp=after)
        for i, (v, t) in enumerate(((x, tail_x), (b, tail_b), (c, tail_c)))
    ]
    for copy in tails:
        copy.start()
    for m in range(3):
        first_hop(m).start()

    @pl.when(home)
    def _():
        for m in range(3):
            src, dst = moves[m][1]
            pltpu.make_async_copy(src.at[0], dst.at[col], w_recv.at[col, m]).start()
            sideways(m, col, src.at[0]).start()

    def send_decay(d, carry):
        target = lax.rem(me + d, n_sp)
        remote(
            dec_src.at[lax.rem(target, pairs)],
            dec_recv.at[d],
            dec_sems.at[0],
            dec_sems.at[1],
            sp=target,
        ).start()
        return carry

    own_decay = pltpu.make_async_copy(
        dec_src.at[lax.rem(me, pairs)], dec_recv.at[0], dec_sems.at[1]
    )
    own_decay.start()
    lax.fori_loop(1, n_sp, send_decay, 0)

    keep = [
        jnp.concatenate([pair_columns(jnp.exp(t), j, low_half) for j in range(pairs)], axis=1)
        for t in totals
    ]

    for copy in tails:
        copy.wait()
    has_tail = (me > 0).astype(F32)
    ext_x[0:8, :] = tail_x[...].astype(F32) * has_tail
    ext_b[0:8, :] = tail_b[...].astype(F32) * has_tail
    inputs_of_block(0)

    for i in range(STATE_WIDTH // 16):
        for j in range(pairs):
            lanes = slice(128 * j, 128 * (j + 1))
            state = added[0, 16 * i : 16 * (i + 1), lanes]
            for k in range(1, n_blocks):
                state = keep[k][:, lanes] * state + added[k, 16 * i : 16 * (i + 1), lanes]
            sl_src[pairs * i + j] = state.astype(BF16)

    def send_slice(d, carry):
        target = lax.rem(me + d, n_sp)
        remote(sl_src.at[target], sl_recv.at[d], sl_sems.at[0], sl_sems.at[1], sp=target).start()
        return carry

    own_slice = pltpu.make_async_copy(sl_src.at[me], sl_recv.at[0], sl_sems.at[1])
    own_slice.start()
    lax.fori_loop(1, n_sp, send_slice, 0)

    for i in (8, 11, 3):
        loads[i].wait()
    ext_c[8:, :] = c[...].astype(F32)
    ext_c[0:8, :] = tail_c[...].astype(F32) * has_tail
    for k in range(n_blocks):
        rows = slice(BLOCK * k, BLOCK * (k + 1))
        across = running[k].T
        grown = jnp.exp(running[k])
        for g in range(groups):
            lanes_g = slice(128 * g, 128 * (g + 1))
            cc[rows, lanes_g] = conv(ext_c, fc, k, g).astype(BF16)
            products = dot(cc[rows, lanes_g], cb[rows, lanes_g], ((1,), (1,)))
            for j in range(g * pairs // groups, (g + 1) * pairs // groups):
                lanes = slice(128 * j, 128 * (j + 1))
                weighed = []
                for h in (2 * j, 2 * j + 1):
                    spread = running[k][:, h : h + 1] - across[h : h + 1, :]
                    factors = jnp.exp(jnp.where(causal, spread, -jnp.inf))
                    weighed.append((products * factors).astype(BF16))
                value = ysg[rows, lanes]
                inputs = (value * pair_columns(steps[rows], j, low_half)).astype(BF16)
                zero = jnp.zeros_like(inputs)
                stacked = jnp.concatenate(
                    [jnp.where(low_half, inputs, zero), jnp.where(low_half, zero, inputs)], axis=0
                )
                within = dot(jnp.concatenate(weighed, axis=1), stacked)
                opened = silu(gate[rows, lanes].astype(F32))
                passed = value * pair_columns(direct[...], j, low_half)
                ysg[rows, lanes] = (passed + within) * opened
                ersg[rows, lanes] = pair_columns(grown, j, low_half) * opened

    pltpu.make_async_copy(dec_recv, dec_recv, dec_sems.at[1]).wait()
    pltpu.make_async_copy(sl_recv, sl_recv, sl_sems.at[1]).wait()

    def scan_step(j, state):
        d = lax.rem(me - j + n_sp, n_sp)
        pf_src[j] = state.astype(BF16)
        return jnp.exp(dec_recv[d]) * state + sl_recv[d].astype(F32)

    lax.fori_loop(0, n_sp, scan_step, jnp.zeros((16, 128), F32))

    def send_prefix(d, carry):
        target = lax.rem(me + d, n_sp)
        remote(pf_src.at[target], pf_recv.at[me], pf_sems.at[0], pf_sems.at[1], sp=target).start()
        return carry

    own_prefix = pltpu.make_async_copy(pf_src.at[me], pf_recv.at[me], pf_sems.at[1])
    own_prefix.start()
    lax.fori_loop(1, n_sp, send_prefix, 0)
    for i in (12, 20, 13, 14, 15, 16, 17, 18, 19):
        loads[i].wait()

    named = routes[...].astype(F32).T.astype(jnp.int32)
    distance = lax.shift_right_logical(named, 1) - chip
    distance = jnp.where(distance < 0, distance + n_chips, distance)
    near = lax.shift_right_logical(distance, 2)
    block = 4 * near + 2 * (distance & 1) + jnp.where((named & 1) == lax.div(col, 2), 0, 1)
    block = block + (n_sp // 2) * lax.shift_right_logical(distance & 3, 1)
    shares = weights[...].T
    expert_id = lax.broadcasted_iota(jnp.int32, (n_rows, n_sp), 1)
    hits = [(expert_id == block[:, k : k + 1]).astype(F32) for k in range(2)]
    r_id = lax.broadcasted_iota(jnp.int32, (n_rows, n_rows), 0)
    s_id = lax.broadcasted_iota(jnp.int32, (n_rows, n_rows), 1)
    before = dot((s_id < r_id).astype(BF16), (hits[0] + hits[1]).astype(BF16))
    slot_id = lax.broadcasted_iota(jnp.int32, (n_rows, slots), 1)
    at_slot = []
    for k in range(2):
        rank = jnp.sum(before * hits[k], axis=1, keepdims=True).astype(jnp.int32)
        at_slot.append(slot_id == block[:, k : k + 1] * cap + rank)
    chosen = (at_slot[0] | at_slot[1]).astype(F32).astype(BF16)
    share = jnp.where(at_slot[0], shares[:, 0:1], 0.0) + jnp.where(at_slot[1], shares[:, 1:2], 0.0)
    coarse = share.astype(BF16)
    fine = (share - coarse.astype(F32)).astype(BF16)
    gain = gns[...].astype(F32).reshape(1, width)

    pltpu.make_async_copy(pf_recv, pf_recv, pf_sems.at[1]).wait()

    incoming = jnp.concatenate(
        [
            jnp.concatenate([pf_recv[pairs * i + j] for j in range(pairs)], axis=1)
            for i in range(STATE_WIDTH // 16)
        ],
        axis=0,
    ).astype(F32)
    for k in range(n_blocks):
        rows = slice(BLOCK * k, BLOCK * (k + 1))
        for g in range(groups):
            lanes = slice(group_width * g, group_width * (g + 1))
            carried = dot(cc[rows, 128 * g : 128 * (g + 1)], incoming[:, lanes].astype(BF16))
            gated = ysg[rows, lanes] + carried * ersg[rows, lanes]
            power = jnp.mean(gated * gated, axis=-1, keepdims=True)
            rows_out[rows, lanes] = (gated * lax.rsqrt(power + EPS) * gain[:, lanes]).astype(BF16)
        if k + 1 < n_blocks:
            incoming = keep[k] * incoming + added[k]

    part = length // n_tp
    half = part // 2
    right, left = lax.rem(col + 1, n_tp), lax.rem(col + n_tp - 1, n_tp)
    opposite = lax.rem(col + 2, n_tp)

    def project(target):
        start = pl.multiple_of(target * part, part)
        for q in range(4):
            lanes = slice(512 * q, 512 * (q + 1))
            partial[pl.ds(start, part), lanes] = dot(
                rows_out[pl.ds(start, part), :], wout[:, lanes]
            ).astype(BF16)

    def half_of(target, which):
        return pl.ds(pl.multiple_of(target * part + which * half, half), half)

    def pass_on(i, rows, dst, target):
        return remote(
            partial.at[rows], dst, tp_sems.at[0, i], tp_sems.at[1, i], tp=target
        )

    project(opposite)
    outward = [
        pass_on(0, half_of(opposite, 0), relayed.at[0], right),
        pass_on(1, half_of(opposite, 1), relayed.at[1], left),
    ]
    for copy in outward:
        copy.start()
    project(right)
    direct_right = pass_on(2, half_of(right, 1), arrived.at[0], right)
    direct_right.start()
    project(left)
    direct_left = pass_on(3, half_of(left, 0), arrived.at[1], left)
    direct_left.start()
    outward[0].wait()
    rows = half_of(right, 0)
    partial[rows, :] = (partial[rows, :].astype(F32) + relayed[0].astype(F32)).astype(BF16)
    joined_right = pass_on(4, rows, arrived.at[2], right)
    joined_right.start()
    outward[1].wait()
    rows = half_of(left, 1)
    partial[rows, :] = (partial[rows, :].astype(F32) + relayed[1].astype(F32)).astype(BF16)
    joined_left = pass_on(5, rows, arrived.at[3], left)
    joined_left.start()
    project(col)

    @pl.when(home)
    def _():
        for m in range(3):
            arrival(m, across_x).wait()
            relay(m).start()
            sideways(m, across_x).start()
            arrival(m, beside).wait()
            sideways(m, beside).start()

    for copy in (direct_right, direct_left, joined_right, joined_left):
        copy.wait()
    for which in range(2):
        rows = half_of(col, which)
        span = slice(half * which, half * (which + 1))
        mixed = partial[rows, :].astype(F32)
        mixed = mixed + arrived[1 - which].astype(F32) + arrived[2 + which].astype(F32)
        mid[span, :] = layer_norm(
            ALPHA * resid[span, :].astype(F32) + mixed, n1s[...], n1b[...]
        ).astype(BF16)

    for q in range(4):
        lanes = slice(512 * q, 512 * (q + 1))
        piece = dot(chosen, mid[:, lanes], ((0,), (0,))).astype(BF16)
        outgoing[:, 4 * q : 4 * (q + 1), :] = piece.reshape(slots, 4, 128)

    def place_of(d):
        r = lax.rem(d, n_sp // 2)
        quarter = 4 * lax.div(r, 4) + 2 * lax.div(d, n_sp // 2) + lax.rem(lax.div(r, 2), 2)
        return quarter, col + lax.rem(d, 2) * (across_x - col)

    n_parts = 2
    blocks = n_sp // n_parts
    piece_rows = blocks * cap

    def send_tokens(d, carry):
        quarter, plane = place_of(d)
        span = pl.ds(cap * d, cap)
        remote(
            outgoing.at[span],
            received.at[span],
            there.at[0],
            there.at[1 + lax.div(d, blocks)],
            sp=2 * lax.rem(chip + quarter, n_chips) + core,
            tp=plane,
        ).start()
        return carry

    def send_answers(d, carry):
        quarter, plane = place_of(d)
        span = pl.ds(cap * d, cap)
        remote(
            answers.at[span],
            returned.at[span],
            back.at[0],
            back.at[1],
            sp=2 * lax.rem(chip - quarter + n_chips, n_chips) + core,
            tp=plane,
        ).start()
        return carry

    own = pltpu.make_async_copy(outgoing.at[pl.ds(0, cap)], received.at[pl.ds(0, cap)], there.at[1])
    own.start()
    lax.fori_loop(1, n_sp, send_tokens, 0)

    def hidden_part(place):
        opened = dot(tokens[...], wg_v[place])
        upward = dot(tokens[...], wu_v[place])
        hidden[place] = (silu(opened) * upward).astype(BF16)

    early = (col, beside, across_x)

    def early_place(i):
        return jnp.where(i == 0, early[0], jnp.where(i == 1, early[1], early[2]))

    def early_hidden(i, carry):
        hidden_part(early_place(i))
        return carry

    def down(place, rows):
        return dot(hidden[place], wd_v[place, rows, :], ((1,), (1,)))

    def early_down():
        def chunk(q, carry):
            rows = pl.ds(pl.multiple_of(256 * q, 256), 256)
            total = down(early[0], rows) + down(early[1], rows) + down(early[2], rows)
            summed[q] = total
            return carry

        lax.fori_loop(0, features // 256, chunk, 0)

    def late_down(first_row):
        for q in range(features // 256):
            total = summed[q] + down(last_place, slice(256 * q, 256 * (q + 1)))
            answers[first_row : first_row + piece_rows, 2 * q : 2 * q + 2, :] = total.astype(
                BF16
            ).reshape(piece_rows, 2, 128)

    @pl.when(home)
    def _():
        for m in range(3):
            arrival(m, col).wait()

    @pl.when(jnp.logical_not(home))
    def _():
        for m in range(3):
            for place in early:
                arrival(m, place).wait()

    for p in range(n_parts):
        span = pl.ds(piece_rows * p, piece_rows)
        pltpu.make_async_copy(received.at[span], received.at[span], there.at[1 + p]).wait()
        tokens[...] = received[span].reshape(piece_rows, features)
        lax.fori_loop(0, 3, early_hidden, 0)
        early_down()
        if p == 0:
            for m in range(3):
                arrival(m, last_place).wait()

                @pl.when(home)
                def _():
                    sideways(m, last_place).start()

        hidden_part(last_place)
        late_down(piece_rows * p)
        if p == 0:
            own = pltpu.make_async_copy(
                answers.at[pl.ds(0, cap)], returned.at[pl.ds(0, cap)], back.at[1]
            )
            own.start()
        lax.fori_loop(max(1, blocks * p), blocks * (p + 1), send_answers, 0)

    pltpu.make_async_copy(returned, returned, back.at[1]).wait()
    back_rows = returned[...].reshape(slots, features)
    ffn = dot(coarse, back_rows) + dot(fine, back_rows)
    out[...] = layer_norm(ALPHA * mid[...].astype(F32) + ffn, n2s[...], n2b[...]).astype(BF16)

    def wait_sent(src, sem):
        remote(src, src, sem, sem, sp=after).wait_send()

    wait_sent(dec_recv.at[pl.ds(0, n_sp - 1)], dec_sems.at[0])
    wait_sent(sl_src.at[pl.ds(0, n_sp - 1)], sl_sems.at[0])
    wait_sent(pf_src.at[pl.ds(0, n_sp - 1)], pf_sems.at[0])
    rest = pl.ds(cap, slots - cap)
    wait_sent(outgoing.at[rest], there.at[0])
    wait_sent(answers.at[rest], back.at[0])
    for m in range(3):
        first_hop(m).wait_send()

    @pl.when(home)
    def _():
        for m in range(3):
            relay(m).wait_send()
            for place in range(n_tp):
                sideways(m, place).wait_send()


def shards(n_sp, n_tp, *arguments):
    (
        head_input_values,
        group_input_vectors,
        group_readout_vectors,
        output_gate_values,
        step_size_logits,
        extra_log_decay,
        head_input_filter,
        input_vector_filter,
        readout_vector_filter,
        step_size_bias,
        head_rate_logarithm,
        direct_path_weight,
        group_norm_scale,
        mixer_output_weight,
        residual,
        first_norm_scale,
        first_norm_bias,
        routes,
        routing_weight,
        expert_gate_weight,
        expert_up_weight,
        expert_down_weight,
        final_norm_scale,
        final_norm_bias,
    ) = arguments
    length, width = head_input_values.shape
    state_lanes = group_input_vectors.shape[1]
    rows_here, features = residual.shape
    n_blocks = length // BLOCK
    pairs = width // 128
    slices = (n_sp, 16, 128)
    vmem = pl.BlockSpec(memory_space=pltpu.VMEM)
    anywhere = pl.BlockSpec(memory_space=pl.ANY)
    dma = pltpu.SemaphoreType.DMA
    experts = n_sp * expert_gate_weight.shape[0]
    cap = max(2, rows_here * routes.shape[1] * 5 // (3 * experts))
    slots = n_sp * cap
    tiles = (slots, features // 128, 128)
    part = expert_gate_weight.shape[2]
    operands = (
        head_input_values,
        group_input_vectors,
        group_readout_vectors,
        output_gate_values,
        step_size_logits.T,
        extra_log_decay.T,
        head_input_filter,
        input_vector_filter,
        readout_vector_filter,
        step_size_bias.reshape(1, -1),
        head_rate_logarithm.reshape(1, -1),
        direct_path_weight.reshape(1, -1),
        group_norm_scale,
        residual,
        first_norm_scale.reshape(1, -1),
        first_norm_bias.reshape(1, -1),
        routes.T,
        routing_weight.T,
        final_norm_scale.reshape(1, -1),
        final_norm_bias.reshape(1, -1),
        mixer_output_weight,
        expert_gate_weight,
        expert_up_weight,
        expert_down_weight,
    )
    return pl.pallas_call(
        functools.partial(fused_kernel, n_sp, n_tp, cap),
        out_shape=jax.ShapeDtypeStruct((rows_here, features), BF16),
        in_specs=[anywhere] * len(operands),
        out_specs=vmem,
        scratch_shapes=[
            *(pltpu.VMEM(v.shape, v.dtype) for v in operands[:21]),
            pltpu.VMEM((8, width), BF16),
            pltpu.VMEM((8, state_lanes), BF16),
            pltpu.VMEM((8, state_lanes), BF16),
            pltpu.VMEM((length + 8, width), F32),
            pltpu.VMEM((length + 8, state_lanes), F32),
            pltpu.VMEM((length + 8, state_lanes), F32),
            pltpu.VMEM((pairs, 1, 128), F32),
            pltpu.VMEM((n_sp, 1, 128), F32),
            pltpu.VMEM(slices, BF16),
            pltpu.VMEM(slices, BF16),
            pltpu.VMEM(slices, BF16),
            pltpu.VMEM(slices, BF16),
            pltpu.VMEM((length, width), BF16),
            pltpu.VMEM((length, width), BF16),
            pltpu.VMEM((length, state_lanes), BF16),
            pltpu.VMEM((length, state_lanes), BF16),
            pltpu.VMEM((length, width), F32),
            pltpu.VMEM((length, width), F32),
            pltpu.VMEM((n_blocks, STATE_WIDTH, width), F32),
            pltpu.VMEM((length, width), BF16),
            pltpu.VMEM((length, features), BF16),
            pltpu.VMEM((2, rows_here // 2, features), BF16),
            pltpu.VMEM((4, rows_here // 2, features), BF16),
            pltpu.VMEM((rows_here, features), BF16),
            pltpu.VMEM(tiles, BF16),
            pltpu.VMEM(tiles, BF16),
            pltpu.VMEM(tiles, BF16),
            pltpu.VMEM(tiles, BF16),
            pltpu.VMEM((slots // 2, features), BF16),
            pltpu.VMEM((n_tp, slots // 2, part), BF16),
            pltpu.VMEM((features // 256, slots // 2, 256), F32),
            pltpu.VMEM((n_tp, features, part), BF16),
            pltpu.VMEM((n_tp, features, part), BF16),
            pltpu.VMEM((n_tp, features, part), BF16),
            dma((21,)),
            dma((2, 3)),
            dma((2,)),
            dma((2,)),
            dma((2,)),
            dma((2, 6)),
            dma((3,)),
            dma((n_tp, 3)),
            dma((3,)),
            dma((n_tp, 3)),
            dma((3,)),
            dma((2,)),
        ],
        compiler_params=pltpu.CompilerParams(
            vmem_limit_bytes=VMEM_LIMIT, has_side_effects=True, collective_id=0
        ),
        name="fused",
    )(*operands)


def solution(mesh):
    every = P(("sp", "tp"), None)
    placed = (
        *([P("sp", "tp")] * 6),
        *([P(None, "tp")] * 3),
        *([P("tp")] * 4),
        P("tp", None),
        every,
        P(),
        P(),
        every,
        every,
        *([P("sp", None, "tp")] * 3),
        P(),
        P(),
    )
    return jax.shard_map(
        functools.partial(shards, mesh.shape["sp"], mesh.shape["tp"]),
        mesh=mesh,
        in_specs=placed,
        out_specs=every,
        check_vma=False,
    )
```

time: 151 us -> 134 us (0.89)
  Pallas kernels: 149 us -> 133 us
    pallas_call x1, Pallas kernels: 149 us -> 133 us  [shards(): pl.pallas_call(functools.partial(fused_kernel, n_sp, n_tp, cap), out_shap...]
where the time goes in v3:
time: 134 us
  Pallas kernels  133 us (99%)
  local copies, waits for them, and re-layouts  1.77 us (1%)
    pallas_call x1, Pallas kernels, shards(): pl.pallas_call(functools.partial(fused_kernel, n_sp, n_tp, cap), out_shap...  133 us

profile of v3, /device:TPU:1, one launch (start us, length us, event | category | flops | bytes accessed | tf_op | source)
XLA Modules:
  0.0 134.3 jit_solution(7814180817052457035)
XLA Ops:
  0.0 132.6 %fused.1 = bf16[96,2048]{1,0:T(8,128)(2,1)} custom-call(bf16[384,1024]{1,0:T(8,128)(2,1)} %refs_0_.1, bf16[384,256]{1,0:T(8,128)(2,1)} %refs_1_.1, bf16[384,256]{1,0:T(8,128)(2,1)} %refs_2_.1, bf16[384,1024]{1,0:T(8,128)(2,1)} %refs_3_.1, f32[16,384]{1,0:T(8,128)} %bitcast.11, f32[16,384]{1,0:T(8,128)} %bitcast.12, bf16[4,1024]{1,0:T(4,128)(2,1)} %refs_6_.1, ...), custom_call_target="tpu_custom_call" | custom-call | tf_op jit(solution)/shard_map/fused/pallas_call | solution.py:664
  132.6 1.8 %copy.26 = bf16[96,2048]{1,0:T(8,128)(2,1)} copy(bf16[96,2048]{1,0:T(8,128)(2,1)} %fused.1) | data formatting | bytes 786432

commit v4 on v3

--- a/solution.py
+++ b/solution.py
@@ -98,6 +98,7 @@
         wg_v,
         wu_v,
         wd_v,
+        detour,
         load_sems,
         tail_sems,
         dec_sems,
@@ -108,6 +109,7 @@
         w_recv,
         w_relay,
         w_side,
+        w_help,
         there,
         back,
     ) = refs
@@ -116,11 +118,21 @@
     core = lax.rem(me, 2)
     chip = lax.div(me, 2)
     n_chips = n_sp // 2
-    beside = col + 1 - 2 * lax.rem(col, 2)
-    across_x = n_tp - 1 - col
-    last_place = n_tp - 1 - beside
+    parity = lax.rem(chip, 2)
     sibling = me + 1 - 2 * core
-    home = lax.div(col, 2) == core
+    helper = 2 * (chip + 1 - 2 * parity) + core
+
+    def roles(shift):
+        role = lax.rem(col + shift, n_tp)
+        partner = role + 1 - 2 * lax.rem(role, 2)
+        places = [lax.rem(r - shift + n_tp, n_tp) for r in (partner, 3 - role, 3 - partner)]
+        return lax.div(role, 2) == core, *places
+
+    home, beside, across_x, last_place = roles(parity)
+    helps, helped_beside, helped_place, _ = roles(1 - parity)
+
+    def crossed(shift):
+        return lax.rem(3 - col - 2 * shift + n_tp, n_tp)
     moves = tuple(enumerate(((wg, wg_v), (wu, wu_v), (wd, wd_v))))
     length, width = x.shape
     n_blocks = length // BLOCK
@@ -148,26 +160,53 @@
         return carry
 
     def greet_plane(q, carry):
-        greet(2 * lax.rem(chip + q, n_chips) + core, across_x)
+        greet(2 * lax.rem(chip + q, n_chips) + core, crossed(0))
+        greet(2 * lax.rem(chip + q, n_chips) + core, crossed(1))
         return carry
 
     lax.fori_loop(1, n_sp, greet_column, 0)
     lax.fori_loop(0, n_chips, greet_plane, 0)
-    greet(me, beside)
-    greet(me, last_place)
 
     def arrival(m, place):
         block = moves[m][1][1].at[place]
         return pltpu.make_async_copy(block, block, w_recv.at[place, m])
 
+    ahead = 3 * wg.shape[1] // 8
+
     def first_hop(m):
-        src, dst = moves[m][1]
+        src, dst = moves[min(m, 2)][1]
+        spans = {2: pl.ds(0, ahead), 3: pl.ds(ahead, wg.shape[1] - ahead)}
+        rows = spans.get(m, pl.ds(0, wg.shape[1]))
         target = jnp.where(home, beside, across_x)
-        return remote(src.at[0], dst.at[col], w_first.at[m], w_recv.at[col, m], tp=target)
+        return remote(
+            src.at[0, rows],
+            dst.at[col, rows],
+            w_first.at[m],
+            w_recv.at[col, min(m, 2)],
+            tp=target,
+        )
+
+    cut = wg.shape[1] // 2
+    aside = wg.shape[1] - cut
 
     def relay(m):
-        block = moves[m][1][1].at[across_x]
+        block = moves[m][1][1].at[across_x, pl.ds(0, cut if m < 2 else cut + aside)]
         return remote(block, block, w_relay.at[m], w_recv.at[across_x, m], tp=beside)
+
+    def to_helper(m):
+        block = moves[m][1][1].at[across_x, pl.ds(cut, aside)]
+        return remote(block, detour.at[m], w_help.at[0, m], w_help.at[1, m], sp=helper)
+
+    def help_on(m):
+        block = moves[m][1][1].at[helped_place, pl.ds(cut, aside)]
+        return remote(
+            detour.at[m],
+            block,
+            w_help.at[2, m],
+            w_recv.at[helped_place, m],
+            sp=helper,
+            tp=helped_beside,
+        )
 
     def sideways(m, place, src=None):
         block = moves[m][1][1].at[place]
@@ -178,6 +217,17 @@
             w_recv.at[place, m],
             sp=sibling,
         )
+
+    def start_weights(first, last):
+        for m in range(first, last):
+            first_hop(m).start()
+
+        @pl.when(home)
+        def _():
+            for m in range(first, last):
+                src, dst = moves[m][1]
+                pltpu.make_async_copy(src.at[0], dst.at[col], w_recv.at[col, m]).start()
+                sideways(m, col, src.at[0]).start()
 
     low_half = lax.broadcasted_iota(jnp.int32, (BLOCK, 128), 1) < 64
     row_id = lax.broadcasted_iota(jnp.int32, (BLOCK, BLOCK), 0)
@@ -233,7 +283,7 @@
         inputs_of_block(k)
 
     loads[2].wait()
-    pl.semaphore_wait(barrier, n_sp - 1 + n_chips + 2)
+    pl.semaphore_wait(barrier, n_sp - 1 + 2 * n_chips)
     after = lax.rem(me + 1, n_sp)
     tails = [
         remote(v.at[pl.ds(length - 8, 8)], t, tail_sems.at[0, i], tail_sems.at[1, i], sp=after)
@@ -241,16 +291,7 @@
     ]
     for copy in tails:
         copy.start()
-    for m in range(3):
-        first_hop(m).start()
-
-    @pl.when(home)
-    def _():
-        for m in range(3):
-            src, dst = moves[m][1]
-            pltpu.make_async_copy(src.at[0], dst.at[col], w_recv.at[col, m]).start()
-            sideways(m, col, src.at[0]).start()
-
+    start_weights(0, 3)
     def send_decay(d, carry):
         target = lax.rem(me + d, n_sp)
         remote(
@@ -353,7 +394,9 @@
     distance = lax.shift_right_logical(named, 1) - chip
     distance = jnp.where(distance < 0, distance + n_chips, distance)
     near = lax.shift_right_logical(distance, 2)
-    block = 4 * near + 2 * (distance & 1) + jnp.where((named & 1) == lax.div(col, 2), 0, 1)
+    role = (col + (lax.shift_right_logical(named, 1) & 1)) & 3
+    block = 4 * near + 2 * (distance & 1)
+    block = block + jnp.where((named & 1) == lax.shift_right_logical(role, 1), 0, 1)
     block = block + (n_sp // 2) * lax.shift_right_logical(distance & 3, 1)
     shares = weights[...].T
     expert_id = lax.broadcasted_iota(jnp.int32, (n_rows, n_sp), 1)
@@ -391,6 +434,12 @@
             rows_out[rows, lanes] = (gated * lax.rsqrt(power + EPS) * gain[:, lanes]).astype(BF16)
         if k + 1 < n_blocks:
             incoming = keep[k] * incoming + added[k]
+
+    @pl.when(home)
+    def _():
+        for m in range(2):
+            arrival(m, across_x).wait()
+            to_helper(m).start()
 
     part = length // n_tp
     half = part // 2
@@ -436,16 +485,27 @@
     partial[rows, :] = (partial[rows, :].astype(F32) + relayed[1].astype(F32)).astype(BF16)
     joined_left = pass_on(5, rows, arrived.at[3], left)
     joined_left.start()
+    first_hop(3).start()
     project(col)
 
-    @pl.when(home)
-    def _():
-        for m in range(3):
-            arrival(m, across_x).wait()
-            relay(m).start()
-            sideways(m, across_x).start()
-            arrival(m, beside).wait()
-            sideways(m, beside).start()
+    def pass_weights(first, last):
+        @pl.when(home)
+        def _():
+            for m in range(first, last):
+                if m == 2:
+                    arrival(m, across_x).wait()
+                relay(m).start()
+                sideways(m, across_x).start()
+                arrival(m, beside).wait()
+                sideways(m, beside).start()
+
+    def help_with(m):
+        @pl.when(helps)
+        def _():
+            to_helper(m).wait_recv()
+            help_on(m).start()
+
+    pass_weights(0, 2)
 
     for copy in (direct_right, direct_left, joined_right, joined_left):
         copy.wait()
@@ -466,27 +526,31 @@
     def place_of(d):
         r = lax.rem(d, n_sp // 2)
         quarter = 4 * lax.div(r, 4) + 2 * lax.div(d, n_sp // 2) + lax.rem(lax.div(r, 2), 2)
-        return quarter, col + lax.rem(d, 2) * (across_x - col)
+        return quarter, lax.rem(d, 2)
+
+    def plane(crossing, shift):
+        return col + crossing * (crossed(shift) - col)
 
     n_parts = 2
     blocks = n_sp // n_parts
     piece_rows = blocks * cap
 
     def send_tokens(d, carry):
-        quarter, plane = place_of(d)
+        quarter, crossing = place_of(d)
+        target = lax.rem(chip + quarter, n_chips)
         span = pl.ds(cap * d, cap)
         remote(
             outgoing.at[span],
             received.at[span],
             there.at[0],
             there.at[1 + lax.div(d, blocks)],
-            sp=2 * lax.rem(chip + quarter, n_chips) + core,
-            tp=plane,
+            sp=2 * target + core,
+            tp=plane(crossing, lax.rem(target, 2)),
         ).start()
         return carry
 
     def send_answers(d, carry):
-        quarter, plane = place_of(d)
+        quarter, crossing = place_of(d)
         span = pl.ds(cap * d, cap)
         remote(
             answers.at[span],
@@ -494,7 +558,7 @@
             back.at[0],
             back.at[1],
             sp=2 * lax.rem(chip - quarter + n_chips, n_chips) + core,
-            tp=plane,
+            tp=plane(crossing, parity),
         ).start()
         return carry
 
@@ -502,38 +566,42 @@
     own.start()
     lax.fori_loop(1, n_sp, send_tokens, 0)
 
-    def hidden_part(place):
-        opened = dot(tokens[...], wg_v[place])
-        upward = dot(tokens[...], wu_v[place])
-        hidden[place] = (silu(opened) * upward).astype(BF16)
+    def hidden_part(p, place):
+        rows = slice(piece_rows * p, piece_rows * (p + 1))
+        opened = dot(tokens[rows, :], wg_v[place])
+        upward = dot(tokens[rows, :], wu_v[place])
+        hidden[place, rows, :] = (silu(opened) * upward).astype(BF16)
 
     early = (col, beside, across_x)
 
-    def early_place(i):
-        return jnp.where(i == 0, early[0], jnp.where(i == 1, early[1], early[2]))
-
-    def early_hidden(i, carry):
-        hidden_part(early_place(i))
+    def early_hidden(p, i, carry):
+        hidden_part(p, jnp.where(i == 0, early[0], jnp.where(i == 1, early[1], early[2])))
         return carry
 
-    def down(place, rows):
-        return dot(hidden[place], wd_v[place, rows, :], ((1,), (1,)))
-
-    def early_down():
+    def down(p, place, features_here):
+        rows = slice(piece_rows * p, piece_rows * (p + 1))
+        return dot(hidden[place, rows, :], wd_v[place, features_here, :], ((1,), (1,)))
+
+    def early_down(p):
         def chunk(q, carry):
-            rows = pl.ds(pl.multiple_of(256 * q, 256), 256)
-            total = down(early[0], rows) + down(early[1], rows) + down(early[2], rows)
-            summed[q] = total
+            here = pl.ds(pl.multiple_of(256 * q, 256), 256)
+            rows = slice(piece_rows * p, piece_rows * (p + 1))
+            summed[q, rows, :] = functools.reduce(
+                lambda u, v: u + v, [down(p, place, here) for place in early]
+            )
             return carry
 
         lax.fori_loop(0, features // 256, chunk, 0)
 
-    def late_down(first_row):
+    def late_down(p):
+        rows = slice(piece_rows * p, piece_rows * (p + 1))
         for q in range(features // 256):
-            total = summed[q] + down(last_place, slice(256 * q, 256 * (q + 1)))
-            answers[first_row : first_row + piece_rows, 2 * q : 2 * q + 2, :] = total.astype(
-                BF16
-            ).reshape(piece_rows, 2, 128)
+            total = summed[q, rows, :] + down(p, last_place, slice(256 * q, 256 * (q + 1)))
+            answers[rows, 2 * q : 2 * q + 2, :] = total.astype(BF16).reshape(piece_rows, 2, 128)
+
+    help_with(0)
+    help_with(1)
+    pass_weights(2, 3)
 
     @pl.when(home)
     def _():
@@ -546,22 +614,26 @@
             for place in early:
                 arrival(m, place).wait()
 
+    def wait_last(first, last):
+        for m in range(first, last):
+            arrival(m, last_place).wait()
+
+            @pl.when(home)
+            def _():
+                sideways(m, last_place).start()
+
     for p in range(n_parts):
         span = pl.ds(piece_rows * p, piece_rows)
         pltpu.make_async_copy(received.at[span], received.at[span], there.at[1 + p]).wait()
-        tokens[...] = received[span].reshape(piece_rows, features)
-        lax.fori_loop(0, 3, early_hidden, 0)
-        early_down()
+        tokens[span, :] = received[span].reshape(piece_rows, features)
+        lax.fori_loop(0, 3, functools.partial(early_hidden, p), 0)
+        early_down(p)
         if p == 0:
-            for m in range(3):
-                arrival(m, last_place).wait()
-
-                @pl.when(home)
-                def _():
-                    sideways(m, last_place).start()
-
-        hidden_part(last_place)
-        late_down(piece_rows * p)
+            wait_last(0, 2)
+        hidden_part(p, last_place)
+        if p == 0:
+            wait_last(2, 3)
+        late_down(p)
         if p == 0:
             own = pltpu.make_async_copy(
                 answers.at[pl.ds(0, cap)], returned.at[pl.ds(0, cap)], back.at[1]
@@ -583,15 +655,22 @@
     rest = pl.ds(cap, slots - cap)
     wait_sent(outgoing.at[rest], there.at[0])
     wait_sent(answers.at[rest], back.at[0])
-    for m in range(3):
+    for m in range(4):
         first_hop(m).wait_send()
 
     @pl.when(home)
     def _():
         for m in range(3):
             relay(m).wait_send()
+            if m < 2:
+                to_helper(m).wait_send()
             for place in range(n_tp):
                 sideways(m, place).wait_send()
+
+    @pl.when(helps)
+    def _():
+        for m in range(2):
+            help_on(m).wait_send()
 
 
 def shards(n_sp, n_tp, *arguments):
@@ -696,22 +775,24 @@
             pltpu.VMEM(tiles, BF16),
             pltpu.VMEM(tiles, BF16),
             pltpu.VMEM(tiles, BF16),
-            pltpu.VMEM((slots // 2, features), BF16),
-            pltpu.VMEM((n_tp, slots // 2, part), BF16),
-            pltpu.VMEM((features // 256, slots // 2, 256), F32),
+            pltpu.VMEM((slots, features), BF16),
+            pltpu.VMEM((n_tp, slots, part), BF16),
+            pltpu.VMEM((features // 256, slots, 256), F32),
             pltpu.VMEM((n_tp, features, part), BF16),
             pltpu.VMEM((n_tp, features, part), BF16),
             pltpu.VMEM((n_tp, features, part), BF16),
+            pltpu.VMEM((2, features // 2, part), BF16),
             dma((21,)),
             dma((2, 3)),
             dma((2,)),
             dma((2,)),
             dma((2,)),
             dma((2, 6)),
-            dma((3,)),
+            dma((4,)),
             dma((n_tp, 3)),
             dma((3,)),
             dma((n_tp, 3)),
+            dma((3, 2)),
             dma((3,)),
             dma((2,)),
         ],

time: 134 us -> 130 us (0.970)
  Pallas kernels: 133 us -> 128 us
    pallas_call x1, Pallas kernels: 133 us -> 128 us  [shards(): pl.pallas_call(functools.partial(fused_kernel, n_sp, n_tp, cap), out_shap...]
where the time goes in v4:
time: 130 us
  Pallas kernels  128 us (98%)
  local copies, waits for them, and re-layouts  1.77 us (1%)
    pallas_call x1, Pallas kernels, shards(): pl.pallas_call(functools.partial(fused_kernel, n_sp, n_tp, cap), out_shap...  128 us

profile of v4, /device:TPU:1, one launch (start us, length us, event | category | flops | bytes accessed | tf_op | source)
XLA Modules:
  0.0 129.7 jit_solution(17472299833806619675)
XLA Ops:
  0.0 127.9 %fused.1 = bf16[96,2048]{1,0:T(8,128)(2,1)} custom-call(bf16[384,1024]{1,0:T(8,128)(2,1)} %refs_0_.1, bf16[384,256]{1,0:T(8,128)(2,1)} %refs_1_.1, bf16[384,256]{1,0:T(8,128)(2,1)} %refs_2_.1, bf16[384,1024]{1,0:T(8,128)(2,1)} %refs_3_.1, f32[16,384]{1,0:T(8,128)} %bitcast.11, f32[16,384]{1,0:T(8,128)} %bitcast.12, bf16[4,1024]{1,0:T(4,128)(2,1)} %refs_6_.1, ...), custom_call_target="tpu_custom_call" | custom-call | tf_op jit(solution)/shard_map/fused/pallas_call | solution.py:743
  127.9 1.8 %copy.26 = bf16[96,2048]{1,0:T(8,128)(2,1)} copy(bf16[96,2048]{1,0:T(8,128)(2,1)} %fused.1) | data formatting | bytes 786432
